TPU v7x, 32 devices: a whole 2x2x4 slice. The times are simulated.
32 devices in a mesh: sp: 8 (over z, y), tp: 4 (over x, core).
Axes of the slice: x: 2, y: 2, z: 4, core: 2. Of those that a mesh axis runs over, the one named last changes fastest.
Arguments:
- residual: bfloat16 [2048, 2048], P(('sp', 'tp')), may hold values from -6 to 6
- queries: bfloat16 [2048, 2048], P('sp', 'tp'), may hold values from -40 to 40
- key_rows: bfloat16 [2048, 1024], P('sp', 'tp'), may hold values from -40 to 40
- value_rows: bfloat16 [2048, 1024], P('sp', 'tp'), may hold values from -6 to 6
- forget_sums: float32 [2048, 16], P('sp', 'tp'), as said below
- out_weight: bfloat16 [2048, 2048], P('tp'), may hold values from -0.25 to 0.25
- norm_gain: float32 [2048], replicated, may hold values from 0.1 to 1.9
- expert_ids: int32 [2048, 4], P(('sp', 'tp')), may hold values from 0 to 7, all different within a row; in each aligned block of 64 rows (0 to 63, 64 to 127, ...) at most 64 rows name the same one
- route_weights: float32 [2048, 4], P(('sp', 'tp')), may hold values from 0.1 to 1
- expert_gate: bfloat16 [8, 2048, 384], P('sp'), may hold values from -0.125 to 0.125
- expert_up: bfloat16 [8, 2048, 384], P('sp'), may hold values from -0.125 to 0.125
- expert_down: bfloat16 [8, 384, 2048], P('sp'), may hold values from -0.3125 to 0.3125
- shared_gate: bfloat16 [2048, 384], replicated, may hold values from -0.125 to 0.125
- shared_up: bfloat16 [2048, 384], replicated, may hold values from -0.125 to 0.125
- shared_down: bfloat16 [384, 2048], replicated, may hold values from -0.3125 to 0.3125
Outputs:
- layer_out: bfloat16 [2048, 2048], P(('sp', 'tp'))
Inputs may be any that keep to these rules, and one draw needn't show every extreme that they name: `forget_sums`: each head's column never rises from one position to the next. `expert_ids`: each row names 4 different experts; among the rows of one device no expert is named more than 64 times.
All inputs are finite; a program needn't handle non-finite values.
Results may differ from a plain program's by a relative error of at most 0.014.
Values may be sent and summed in bfloat16 or wider, within the bound.
A program may use at most 128 MiB of HBM per device.

v0:
```python
import functools
import math

import jax
import jax.numpy as jnp
from jax import lax
from jax.experimental import pallas as pl
from jax.experimental.pallas import tpu as pltpu
from jax.sharding import PartitionSpec as P

HEADS = 16
KV_HEADS = 8
HEAD_DIM = 128
TOPK = 4


routed_scale = 2.5
norm_eps = 1e-06


MESH_ID = pl.DeviceIdType.MESH
LOG2E = math.log2(math.e)


def remote(src, dst, send_sem, recv_sem, target):
    return pltpu.make_async_remote_copy(
        src_ref=src,
        dst_ref=dst,
        send_sem=send_sem,
        recv_sem=recv_sem,
        device_id=target,
        device_id_type=MESH_ID,
    )


def greet(barrier, target):
    pl.semaphore_signal(barrier, inc=1, device_id=target, device_id_type=MESH_ID)


def attend_kernel(
    enter,
    sp_count,
    score_scale,
    q_ref,
    f_ref,
    k_hbm,
    v_hbm,
    out_ref,
    kbuf,
    vbuf,
    fbuf,
    qs,
    fqs,
    acc,
    top,
    den,
    load_sem,
    up_sem,
    side_sem,
    recv_sem,
):
    me, tp = lax.axis_index("sp"), lax.axis_index("tp")
    line = sp_count // 2
    z, y = me // 2, me % 2
    mate = (2 * z + 1 - y, tp)
    above = (jnp.minimum(me + 2, sp_count - 1), tp)
    below = (jnp.maximum(me - 2, 0), tp)
    bufs = (kbuf, vbuf, fbuf)
    loads = [
        pltpu.make_async_copy(src, buf.at[me], load_sem.at[i])
        for i, (src, buf) in enumerate(zip((k_hbm, v_hbm), bufs))
    ]
    for copy in loads:
        copy.start()
    fbuf[me] = jnp.zeros(fbuf.shape[1:], jnp.float32)
    fbuf[me, : f_ref.shape[0], :] = f_ref[...]
    rows, pair = q_ref.shape[0], qs.shape[1] // q_ref.shape[0]
    kv_heads = qs.shape[0]
    for h in range(kv_heads * pair):
        qs[h // pair, (h % pair) * rows : (h % pair + 1) * rows, :] = q_ref[
            :, h * HEAD_DIM : (h + 1) * HEAD_DIM
        ]
    square = (rows, rows)
    diagonal = lax.broadcasted_iota(jnp.int32, square, 0) == lax.broadcasted_iota(jnp.int32, square, 1)
    for h in range(kv_heads * pair):
        column = jnp.sum(jnp.where(diagonal, f_ref[h : h + 1, :], 0.0), axis=1, keepdims=True)
        fqs[h // pair, (h % pair) * rows : (h % pair + 1) * rows, :] = jnp.broadcast_to(
            column, (rows, HEAD_DIM)
        )
    for copy in loads:
        copy.wait()
    enter()

    def moves(block, step, sems, target):
        return [
            remote(buf.at[block], buf.at[block], sems.at[step, i], recv_sem.at[block, i], target)
            for i, buf in enumerate(bufs)
        ]

    def forward(step, arriving):
        block = 2 * (z - step) + y
        for i in (2, 0, 1):
            if arriving:
                moves(block, step, up_sem, below)[i].wait_recv()

            @pl.when(z < line - 1)
            def _():
                moves(block, step, up_sem, above)[i].start()

            @pl.when(jnp.logical_or(y == 0, step > 0))
            def _():
                moves(block, step, side_sem, mate)[i].start()

    def absorb(block, first):
        for g in range(kv_heads):
            lanes = slice(g * HEAD_DIM, (g + 1) * HEAD_DIM)
            keys, values = kbuf[block, :, lanes], vbuf[block, :, lanes]
            products = lax.dot_general(
                qs[g], keys, (((1,), (1,)), ((), ())), preferred_element_type=jnp.float32
            )
            parts = []
            for j in range(pair):
                h = g * pair + j
                drop = fqs[g, j * rows : (j + 1) * rows, :1] - fbuf[block, h : h + 1, :]
                part = products[j * rows : (j + 1) * rows] * (score_scale * LOG2E) + drop * LOG2E
                if first:
                    at_row = lax.broadcasted_iota(jnp.int32, part.shape, 0)
                    at_col = lax.broadcasted_iota(jnp.int32, part.shape, 1)
                    part = jnp.where(at_row >= at_col, part, -jnp.inf)
                parts.append(part)
            scores = jnp.concatenate(parts, axis=0)
            peak = jnp.max(scores, axis=1, keepdims=True)
            if first:
                weights = jnp.exp2(scores - peak)
                total = jnp.sum(weights, axis=1, keepdims=True)
            else:
                old = top[g][:, :1]
                peak = jnp.maximum(old, peak)
                factor = jnp.exp2(old - peak)
                weights = jnp.exp2(scores - peak)
                total = den[g][:, :1] * factor + jnp.sum(weights, axis=1, keepdims=True)
            mixed = jnp.dot(weights.astype(jnp.bfloat16), values, preferred_element_type=jnp.float32)
            acc[g] = mixed if first else acc[g] * factor + mixed
            top[g] = jnp.broadcast_to(peak, top.shape[1:])
            den[g] = jnp.broadcast_to(total, den.shape[1:])

    forward(0, False)
    absorb(me, True)

    def one_step(step, _):
        @pl.when(step <= z)
        def _():
            block = 2 * (z - step) + y
            forward(step, True)
            absorb(block, False)

        @pl.when(jnp.logical_and(step - 1 <= z, jnp.logical_or(y == 1, step > 1)))
        def _():
            block = 2 * (z - step + 1) + 1 - y
            for copy in moves(block, step - 1, side_sem, mate):
                copy.wait_recv()
            absorb(block, False)

        return 0

    lax.fori_loop(1, line + 1, one_step, 0)
    for g in range(kv_heads):
        done = (acc[g] / den[g]).astype(jnp.bfloat16)
        for j in range(pair):
            h = g * pair + j
            out_ref[:, h * HEAD_DIM : (h + 1) * HEAD_DIM] = done[j * rows : (j + 1) * rows]

    def drain(step, _):
        @pl.when(step <= z)
        def _():
            block = 2 * (z - step) + y

            @pl.when(z < line - 1)
            def _():
                for copy in moves(block, step, up_sem, above):
                    copy.wait_send()

            @pl.when(jnp.logical_or(y == 0, step > 0))
            def _():
                for copy in moves(block, step, side_sem, mate):
                    copy.wait_send()

        return 0

    lax.fori_loop(0, line, drain, 0)


def tail_kernel(
    weights,
    sp_count,
    att_ref,
    res_ref,
    gain_ref,
    ids_ref,
    score_ref,
    wo_hbm,
    eg_hbm,
    eu_hbm,
    ed_hbm,
    sg_hbm,
    su_hbm,
    sd_hbm,
    out_ref,
    wo,
    eg,
    eu,
    ed,
    sg,
    su,
    sd,
    gate_in,
    gate_buf,
    core_out,
    core_in,
    kept,
    x_out,
    x_in,
    base,
    tok,
    side_out,
    side_in,
    own,
    up_out,
    up_in,
    dn_out,
    dn_in,
    load_sem,
    gsend_sem,
    grecv_sem,
    pair_sem,
    hop_sem,
    tok_sem,
    side_send,
    side_recv,
    up_send,
    up_recv,
    dn_send,
    dn_recv,
):
    me, tp = lax.axis_index("sp"), lax.axis_index("tp")
    line = sp_count // 2
    z, y = me // 2, me % 2
    x, c = tp // 2, tp % 2
    mate = (2 * z + 1 - y, tp)
    above = (jnp.minimum(me + 2, sp_count - 1), tp)
    below = (jnp.maximum(me - 2, 0), tp)
    core_mate = (me, 2 * x + 1 - c)
    x_mate = (me, 2 * (1 - x) + c)
    rows = res_ref.shape[0]
    scores = score_ref[...]
    gates = scores / jnp.sum(scores, axis=0, keepdims=True) * routed_scale
    for e in range(sp_count):
        row = jnp.sum(jnp.where(ids_ref[...] == e, gates, 0.0), axis=0, keepdims=True)
        gate_in[e] = jnp.broadcast_to(row, gate_in.shape[1:])
    weights[0].wait()

    def gate_move(j):
        peer, source = lax.rem(me + j, sp_count), me
        return remote(
            gate_in.at[peer], gate_buf.at[source], gsend_sem.at[j - 1], grecv_sem.at[j - 1], (peer, tp)
        )

    def gate_arrival(j):
        source = lax.rem(me - j + sp_count, sp_count)
        return remote(
            gate_in.at[source], gate_buf.at[source], gsend_sem.at[j - 1], grecv_sem.at[j - 1], (source, tp)
        )

    for j in range(1, sp_count):
        gate_move(j).start()

    far, near = (1 - x) * 2, x * 2

    def core_copy(i):
        return remote(core_out.at[i], core_in.at[i], pair_sem.at[0, i], pair_sem.at[1, i], core_mate)

    hop = remote(x_out, x_in, hop_sem.at[0], hop_sem.at[1], x_mate)

    def project(block):
        return jnp.dot(
            att_ref[pl.ds(pl.multiple_of(block * rows, rows), rows), :],
            wo[...],
            preferred_element_type=jnp.float32,
        )

    def project_to(i, _):
        out_x = jnp.where(i == 0, far, near)
        core_out[i] = project(out_x + 1 - c).astype(jnp.bfloat16)
        core_copy(i).start()
        kept[i] = project(out_x + c)
        core_copy(i).wait_recv()
        kept[i] = kept[i] + core_in[i].astype(jnp.float32)

        @pl.when(i == 0)
        def _():
            x_out[...] = kept[0].astype(jnp.bfloat16)
            hop.start()

        return 0

    lax.fori_loop(0, 2, project_to, 0)
    branch = kept[1] + res_ref[...].astype(jnp.float32)
    hop.wait_recv()
    stream = (branch + x_in[...].astype(jnp.float32)).astype(jnp.bfloat16)
    wide = stream.astype(jnp.float32)
    scale = lax.rsqrt(jnp.mean(wide * wide, axis=1, keepdims=True) + norm_eps)
    tok[me] = (wide * scale * gain_ref[...]).astype(jnp.bfloat16)
    base[...] = wide

    halves = 2
    part_rows = rows // halves

    def piece(ref, i, p):
        return ref.at[i, pl.ds(p * part_rows, part_rows), :]

    def tok_move(block, p, sem, target):
        return remote(piece(tok, block, p), piece(tok, block, p), sem, tok_sem.at[block, p], target)

    def block_of(where):
        return 2 * where + y

    def send_up(where, p):
        return tok_move(block_of(where), p, up_send.at[where, p], above)

    def send_dn(where, p):
        return tok_move(block_of(where), p, dn_send.at[where, p], below)

    def send_side(where, p):
        return tok_move(block_of(where), p, side_send.at[where, p], mate)

    for p in range(halves):
        send_side(z, p).start()

        @pl.when(z < line - 1)
        def _():
            send_up(z, p).start()

        @pl.when(z > 0)
        def _():
            send_dn(z, p).start()

    for copy in weights[1:]:
        copy.wait()

    def gated(inputs, gate, up, down):
        first = jnp.dot(inputs, gate[...], preferred_element_type=jnp.float32)
        second = jnp.dot(inputs, up[...], preferred_element_type=jnp.float32)
        hidden = (first / (1.0 + jnp.exp(-first)) * second).astype(jnp.bfloat16)
        return jnp.dot(hidden, down[...], preferred_element_type=jnp.float32)

    base[...] += gated(tok[me], sg, su, sd)
    for j in range(1, sp_count):
        gate_arrival(j).wait_recv()
    gate_buf[me] = gate_in[me]

    def expert(block):
        row = gate_buf[block][:1, :]
        shape = (rows, row.shape[1])
        diagonal = lax.broadcasted_iota(jnp.int32, shape, 0) == lax.broadcasted_iota(jnp.int32, shape, 1)
        column = jnp.sum(jnp.where(diagonal, row, 0.0), axis=1, keepdims=True)
        result = gated(tok[block], eg, eu, ed).astype(jnp.bfloat16).astype(jnp.float32)
        return result * column

    def side_back(where, p):
        return remote(
            piece(side_out, where, p),
            piece(side_in, where, p),
            side_send.at[line + where, p],
            side_recv.at[where, p],
            mate,
        )

    def inside(where):
        return jnp.logical_and(where >= 0, where < line)

    def mates_block(where):
        for p in range(halves):
            tok_move(2 * where + 1 - y, p, side_send.at[where, p], mate).wait_recv()
        side_out[where] = expert(2 * where + 1 - y).astype(jnp.bfloat16)

    def own_part(step):
        def at(i, _):
            where = jnp.where(i == 0, z - step, z + step)

            @pl.when(inside(where))
            def _():
                own[where] = expert(block_of(where))

            return 0

        lax.fori_loop(0, 2, at, 0)

    def mates_part(step):
        def at(i, _):
            where = jnp.where(i == 0, z - step, z + step)

            @pl.when(jnp.logical_and(inside(where), jnp.logical_or(i == 0, step > 0)))
            def _():
                mates_block(where)

            return 0

        lax.fori_loop(0, 2, at, 0)

    own[z] = expert(me)

    def one_step(step, _):
        low, high = z - step, z + step
        for p in range(halves):

            @pl.when(low >= 0)
            def _():
                tok_move(block_of(low), p, up_send.at[low, p], below).wait_recv()
                send_side(low, p).start()

                @pl.when(z < line - 1)
                def _():
                    send_up(low, p).start()

            @pl.when(high < line)
            def _():
                tok_move(block_of(high), p, dn_send.at[high, p], above).wait_recv()
                send_side(high, p).start()

                @pl.when(z > 0)
                def _():
                    send_dn(high, p).start()

        @pl.when(step == line - 1)
        def _():
            for p in range(halves):
                side_back(z, p).start()

        own_part(step)
        mates_part(step - 1)
        return 0

    lax.fori_loop(1, line, one_step, 0)
    mates_part(line - 1)

    def cross(turn, _):
        step = line - 1 - turn
        for where in (z - step, z + step):

            @pl.when(inside(where))
            def _():
                for p in range(halves):
                    side_back(where, p).start()

        return 0

    lax.fori_loop(0, line - 1, cross, 0)

    def up_back(where, p):
        return remote(
            piece(up_out, where, p),
            piece(up_in, where, p),
            up_send.at[line + where, p],
            up_recv.at[where, p],
            above,
        )

    def dn_back(where, p):
        return remote(
            piece(dn_out, where, p),
            piece(dn_in, where, p),
            dn_send.at[line + where, p],
            dn_recv.at[where, p],
            below,
        )

    def back_step(turn, _):
        step = line - 1 - turn % (line - 1)
        upward = (turn < line - 1) == (2 * z < line - 1)
        low, high = z - step, z + step

        def pass_on(where, chained, back, came, leaving):
            for p in range(halves):
                span = pl.ds(p * part_rows, part_rows)
                side_back(where, p).wait_recv()
                leaving[where, span, :] = (
                    own[where, span, :] + side_in[where, span, :].astype(jnp.float32)
                ).astype(jnp.bfloat16)

                @pl.when(chained)
                def _():
                    back(where, p).wait_recv()
                    leaving[where, span, :] = (
                        own[where, span, :]
                        + side_in[where, span, :].astype(jnp.float32)
                        + came[where, span, :].astype(jnp.float32)
                    ).astype(jnp.bfloat16)

                back(where, p).start()

        @pl.when(jnp.logical_and(upward, high < line))
        def _():
            pass_on(high, z > 0, up_back, up_in, up_out)

        @pl.when(jnp.logical_and(jnp.logical_not(upward), low >= 0))
        def _():
            pass_on(low, z < line - 1, dn_back, dn_in, dn_out)

        return 0

    lax.fori_loop(0, 2 * (line - 1), back_step, 0)
    for p in range(halves):
        side_back(z, p).wait_recv()
    base[...] += own[z] + side_in[z].astype(jnp.float32)

    @pl.when(z > 0)
    def _():
        for p in range(halves):
            up_back(z, p).wait_recv()
        base[...] += up_in[z].astype(jnp.float32)

    @pl.when(z < line - 1)
    def _():
        for p in range(halves):
            dn_back(z, p).wait_recv()
        base[...] += dn_in[z].astype(jnp.float32)

    out_ref[...] = base[...].astype(jnp.bfloat16)
    for j in range(1, sp_count):
        gate_move(j).wait_send()
    for i in range(2):
        core_copy(i).wait_send()
    hop.wait_send()

    def drain(where, _):
        for p in range(halves):
            send_side(where, p).wait_send()
            side_back(where, p).wait_send()

            @pl.when(jnp.logical_and(where <= z, z < line - 1))
            def _():
                send_up(where, p).wait_send()

            @pl.when(jnp.logical_and(where >= z, z > 0))
            def _():
                send_dn(where, p).wait_send()

            @pl.when(where > z)
            def _():
                up_back(where, p).wait_send()

            @pl.when(where < z)
            def _():
                dn_back(where, p).wait_send()

        return 0

    lax.fori_loop(0, line, drain, 0)


def layer_kernel(sp_count, score_scale, q_ref, f_ref, k_hbm, v_hbm, res_ref, gain_ref, ids_ref, score_ref, *rest):
    sources, out_ref, rest = rest[:7], rest[7], rest[8:]
    att_ref, attend_scratch, tail_scratch = rest[0], rest[1:13], rest[13:]
    load_sem = tail_scratch[23]
    me, tp = lax.axis_index("sp"), lax.axis_index("tp")
    x, c = tp // 2, tp % 2
    held = tail_scratch[:7]
    weights = [
        pltpu.make_async_copy(sources[i], held[i], load_sem.at[i]) for i in (0, 4, 5, 6, 1, 2, 3)
    ]
    barrier = pltpu.get_barrier_semaphore()
    greet(barrier, (me, 2 * x + 1 - c))
    greet(barrier, (me, 2 * (1 - x) + c))
    for j in range(1, sp_count):
        greet(barrier, (lax.rem(me + j, sp_count), tp))

    def enter():
        pl.semaphore_wait(barrier, sp_count + 1)
        for copy in weights:
            copy.start()

    attend_kernel(enter, sp_count, score_scale, q_ref, f_ref, k_hbm, v_hbm, att_ref, *attend_scratch)
    tail_kernel(
        weights, sp_count, att_ref, res_ref, gain_ref, ids_ref, score_ref, *sources, out_ref, *tail_scratch
    )


def layer_fused(
    residual,
    queries,
    key_rows,
    value_rows,
    forget_sums,
    norm_gain,
    expert_ids,
    route_weights,
    out_weight,
    expert_gate,
    expert_up,
    expert_down,
    shared_gate,
    shared_up,
    shared_down,
    sp_count,
):
    query_rows, heads = queries.shape[0], forget_sums.shape[1]
    kv_heads = key_rows.shape[1] // HEAD_DIM
    stacked = (kv_heads, heads // kv_heads * query_rows, HEAD_DIM)
    rows, width = residual.shape
    line = sp_count // 2
    table = (sp_count, 8, rows)
    vmem, hbm = pl.BlockSpec(memory_space=pltpu.VMEM), pl.BlockSpec(memory_space=pl.ANY)
    bf16, f32 = jnp.bfloat16, jnp.float32
    loaded = (
        out_weight,
        expert_gate[0],
        expert_up[0],
        expert_down[0],
        shared_gate,
        shared_up,
        shared_down,
    )
    dma = pltpu.SemaphoreType.DMA
    one = (rows, width)
    return pl.pallas_call(
        functools.partial(layer_kernel, sp_count, HEAD_DIM ** (-0.5)),
        out_shape=jax.ShapeDtypeStruct(one, bf16),
        in_specs=[vmem, vmem, hbm, hbm] + [vmem] * 4 + [hbm] * 7,
        out_specs=vmem,
        scratch_shapes=[
            pltpu.VMEM(queries.shape, bf16),
            pltpu.VMEM((sp_count,) + key_rows.shape, bf16),
            pltpu.VMEM((sp_count,) + value_rows.shape, bf16),
            pltpu.VMEM((sp_count, -(-heads // 8) * 8, query_rows), f32),
            pltpu.VMEM(stacked, bf16),
            pltpu.VMEM(stacked, f32),
            pltpu.VMEM(stacked, f32),
            pltpu.VMEM(stacked, f32),
            pltpu.VMEM(stacked, f32),
            dma((2,)),
            dma((line, 3)),
            dma((line, 3)),
            dma((sp_count, 3)),
        ]
        + [pltpu.VMEM(w.shape, bf16) for w in loaded]
        + [
            pltpu.VMEM(table, f32),
            pltpu.VMEM(table, f32),
            pltpu.VMEM((2,) + one, bf16),
            pltpu.VMEM((2,) + one, bf16),
            pltpu.VMEM((2,) + one, f32),
            pltpu.VMEM(one, bf16),
            pltpu.VMEM(one, bf16),
            pltpu.VMEM(one, f32),
            pltpu.VMEM((sp_count,) + one, bf16),
            pltpu.VMEM((line,) + one, bf16),
            pltpu.VMEM((line,) + one, bf16),
            pltpu.VMEM((line,) + one, f32),
            pltpu.VMEM((line,) + one, bf16),
            pltpu.VMEM((line,) + one, bf16),
            pltpu.VMEM((line,) + one, bf16),
            pltpu.VMEM((line,) + one, bf16),
            dma((7,)),
            dma((sp_count - 1,)),
            dma((sp_count - 1,)),
            dma((2, 2)),
            dma((2,)),
            dma((sp_count, 2)),
            dma((2 * line, 2)),
            dma((line, 2)),
            dma((2 * line, 2)),
            dma((line, 2)),
            dma((2 * line, 2)),
            dma((line, 2)),
        ],
        compiler_params=pltpu.CompilerParams(
            collective_id=0, has_side_effects=True, vmem_limit_bytes=60 * 2**20
        ),
    )(
        queries,
        forget_sums.T,
        key_rows,
        value_rows,
        residual,
        norm_gain[None, :],
        expert_ids.T,
        route_weights.T,
        *loaded,
    )


def absorb_group(carried, query_group, shard_piece, sum_piece, score_scale):
    query_heads, query_sums, query_pos, last_pos = query_group
    key_piece, value_piece = shard_piece
    piece_rows = key_piece.shape[0]
    query_count, local_kv, group_size, head_size = query_heads.shape
    key_block = math.gcd(piece_rows, 1024)
    key_heads = key_piece.reshape(piece_rows, local_kv, head_size)
    value_heads = value_piece.reshape(piece_rows, local_kv, head_size)
    key_sums = sum_piece.reshape(piece_rows, local_kv, group_size).transpose(1, 2, 0)

    def update(block_start, held):
        row_max, row_sum, weighted = held
        key_part = lax.dynamic_slice_in_dim(key_heads, block_start, key_block, 0)
        value_part = lax.dynamic_slice_in_dim(value_heads, block_start, key_block, 0)
        sums_part = lax.dynamic_slice_in_dim(key_sums, block_start, key_block, 2)
        scores = (
            jnp.einsum("qhgd,khd->hgqk", query_heads, key_part, preferred_element_type=jnp.float32)
            * score_scale
        )
        scores = scores + (query_sums[:, :, :, None] - sums_part[:, :, None, :])
        key_pos = block_start + jnp.arange(key_block, dtype=jnp.int32)
        allowed = query_pos[:, None] >= key_pos[None, :]
        scores = jnp.where(allowed, scores, -jnp.inf)
        new_max = jnp.maximum(row_max, jnp.max(scores, axis=3))
        weights = jnp.exp(scores - new_max[:, :, :, None])
        factor = jnp.exp(row_max - new_max)
        row_sum = row_sum * factor + jnp.sum(weights, axis=3)
        products = jnp.einsum(
            "hgqk,khd->qhgd",
            weights.astype(jnp.bfloat16),
            value_part,
            preferred_element_type=jnp.float32,
        )
        weighted = weighted * factor.transpose(2, 0, 1)[:, :, :, None] + products
        return (new_max, row_sum, weighted)

    def one_block(block_index, held):
        block_start = block_index * key_block
        needed = block_start <= last_pos
        return lax.cond(needed, lambda inner: update(block_start, inner), lambda inner: inner, held)

    return lax.fori_loop(0, piece_rows // key_block, one_block, carried)


def finish(carried):
    row_max, row_sum, weighted = carried
    mixed = weighted / row_sum.transpose(2, 0, 1)[:, :, :, None]
    return mixed.reshape(mixed.shape[0], -1).astype(jnp.bfloat16)


def local(
    residual,
    queries,
    key_rows,
    value_rows,
    forget_sums,
    out_weight,
    norm_gain,
    expert_ids,
    route_weights,
    expert_gate,
    expert_up,
    expert_down,
    shared_gate,
    shared_up,
    shared_down,
):
    sp_count = lax.axis_size("sp")
    sp_index = lax.axis_index("sp")
    local_rows = queries.shape[0]
    local_kv = key_rows.shape[1] // HEAD_DIM
    group_size = HEADS // KV_HEADS
    score_scale = HEAD_DIM ** (-0.5)
    tp_count = lax.axis_size("tp")
    tokens_here = residual.shape[0]
    every_slot = 2 * tokens_here * TOPK >= tokens_here * expert_gate.shape[0] * sp_count
    if every_slot and expert_gate.shape[0] == 1 and sp_count % 2 == 0 and sp_count > 4 and tp_count == 4:
        return layer_fused(
            residual,
            queries,
            key_rows,
            value_rows,
            forget_sums,
            norm_gain,
            expert_ids,
            route_weights,
            out_weight,
            expert_gate,
            expert_up,
            expert_down,
            shared_gate,
            shared_up,
            shared_down,
            sp_count,
        )
    own_first = sp_index * local_rows
    all_sums = lax.all_gather(forget_sums, "sp", axis=0, tiled=True)
    positions = own_first + jnp.arange(local_rows, dtype=jnp.int32)
    groups = [
        (
            queries.reshape(queries.shape[0], local_kv, group_size, HEAD_DIM),
            forget_sums.reshape(forget_sums.shape[0], local_kv, group_size).transpose(1, 2, 0),
            positions,
            positions[-1],
        )
    ]

    def initial(query_count):
        return (
            jnp.full((local_kv, group_size, query_count), -1e30, jnp.float32),
            jnp.zeros((local_kv, group_size, query_count), jnp.float32),
            jnp.zeros((query_count, local_kv, group_size, HEAD_DIM), jnp.float32),
        )

    def absorb(states, shard_piece):
        return tuple(
            (
                absorb_group(held, query_group, shard_piece, all_sums, score_scale)
                for held, query_group in zip(states, groups)
            )
        )

    start_states = tuple((initial(query_group[0].shape[0]) for query_group in groups))
    states = absorb(
        start_states,
        (
            lax.all_gather(key_rows, "sp", axis=0, tiled=True),
            lax.all_gather(value_rows, "sp", axis=0, tiled=True),
        ),
    )
    outputs = [finish(held) for held in states]
    attended = outputs[0]
    rows_out = local_rows // lax.axis_size("tp")
    branch = lax.psum_scatter(
        jnp.dot(attended, out_weight, preferred_element_type=jnp.float32).astype(jnp.bfloat16),
        "tp",
        scatter_dimension=0,
        tiled=True,
    ).astype(jnp.float32)
    stream = (residual.astype(jnp.float32) + branch).astype(jnp.bfloat16)
    wide = lax.optimization_barrier(stream).astype(jnp.float32)
    normed = (
        wide * lax.rsqrt(jnp.mean(wide * wide, axis=1, keepdims=True) + norm_eps) * norm_gain
    ).astype(jnp.bfloat16)
    width = normed.shape[1]
    experts_here = expert_gate.shape[0]
    total_experts = experts_here * sp_count
    capacity = 2 * rows_out * TOPK // total_experts
    flat_ids = expert_ids.reshape(-1)
    assigned = flat_ids.shape[0]
    onehot = (flat_ids[:, None] == jnp.arange(total_experts, dtype=jnp.int32)[None, :]).astype(
        jnp.int32
    )
    slot_rank = jnp.sum((jnp.cumsum(onehot, axis=0) - 1) * onehot, axis=1)
    target = flat_ids * capacity + slot_rank
    slot_count = total_experts * capacity
    source = (
        jnp.full((slot_count,), assigned, jnp.int32)
        .at[target]
        .set(jnp.arange(assigned, dtype=jnp.int32))
    )
    padded = jnp.concatenate([normed, jnp.zeros((1, width), jnp.bfloat16)], axis=0)
    outgoing = padded[source // TOPK].reshape(sp_count, experts_here, capacity, width)
    arrived = lax.all_to_all(outgoing, "sp", split_axis=0, concat_axis=0, tiled=True)
    gate_part = jnp.einsum(
        "necd,edf->necf", arrived, expert_gate, preferred_element_type=jnp.float32
    )
    up_part = jnp.einsum("necd,edf->necf", arrived, expert_up, preferred_element_type=jnp.float32)
    hidden = (jax.nn.silu(gate_part) * up_part).astype(jnp.bfloat16)
    processed = jnp.einsum(
        "necf,efd->necd", hidden, expert_down, preferred_element_type=jnp.float32
    ).astype(jnp.bfloat16)
    returned = lax.all_to_all(processed, "sp", split_axis=0, concat_axis=0, tiled=True)
    results = returned.reshape(slot_count, width)
    picked = results[target].reshape(rows_out, TOPK, width).astype(jnp.float32)
    gates = route_weights / jnp.sum(route_weights, axis=1, keepdims=True) * routed_scale
    routed = jnp.sum(gates[:, :, None] * picked, axis=1)
    shared_hidden = (
        jax.nn.silu(jnp.dot(normed, shared_gate, preferred_element_type=jnp.float32))
        * jnp.dot(normed, shared_up, preferred_element_type=jnp.float32)
    ).astype(jnp.bfloat16)
    shared_out = jnp.dot(shared_hidden, shared_down, preferred_element_type=jnp.float32)
    return (wide + shared_out + routed).astype(jnp.bfloat16)


def solution(mesh):
    in_specs = (
        P(("sp", "tp"), None),
        P("sp", "tp"),
        P("sp", "tp"),
        P("sp", "tp"),
        P("sp", "tp"),
        P("tp", None),
        P(),
        P(("sp", "tp"), None),
        P(("sp", "tp"), None),
        P("sp", None, None),
        P("sp", None, None),
        P("sp", None, None),
        P(),
        P(),
        P(),
    )
    out_specs = P(("sp", "tp"), None)
    return jax.shard_map(local, mesh=mesh, in_specs=in_specs, out_specs=out_specs, check_vma=False)
```

profile of v0, /device:TPU:24, one launch (start us, length us, event | category | flops | bytes accessed | tf_op | source)
XLA Modules:
  0.0 96.6 jit_solution(13948936968205842023)
XLA Ops:
  0.0 94.9 %shard_map.145 = bf16[64,2048]{1,0:T(8,128)(2,1)} custom-call(bf16[256,512]{1,0:T(8,128)(2,1)} %q_ref.1, f32[4,256]{1,0:T(4,128)} %bitcast.11, bf16[256,256]{1,0:T(8,128)(2,1)} %k_hbm.1, bf16[256,256]{1,0:T(8,128)(2,1)} %v_hbm.1, bf16[64,2048]{1,0:T(8,128)(2,1)} %res_ref.1, f32[1,2048]{1,0:T(1,128)} %bitcast.10, s32[4,64]{1,0:T(4,128)} %bitcast.12, ...), custom_call_target="tpu_custom_call" | custom-call | tf_op jit(solution)/shard_map/pallas_call | solution.py:625
  95.0 1.7 %copy.17 = bf16[64,2048]{1,0:T(8,128)(2,1)} copy(bf16[64,2048]{1,0:T(8,128)(2,1)} %shard_map.145) | data formatting | bytes 524288
where the time goes:
time: 96.8 us; the launch traced here: 96.6 us
  Pallas kernels  94.9 us (98%)
  local copies, waits for them, and re-layouts  1.67 us (2%)
    pallas_call x1, Pallas kernels, layer_fused(): pl.pallas_call(functools.partial(layer_kernel, sp_count, HEAD_DIM ** (-0....  94.9 us

commit v1 on v0

v1 whole, which is shorter than its diff:
```python
import functools
import math
import types

import jax
import jax.numpy as jnp
from jax import lax
from jax.experimental import pallas as pl
from jax.experimental.pallas import tpu as pltpu
from jax.sharding import PartitionSpec as P

HEADS = 16
KV_HEADS = 8
HEAD_DIM = 128
TOPK = 4


routed_scale = 2.5
norm_eps = 1e-06


MESH_ID = pl.DeviceIdType.MESH
LOG2E = math.log2(math.e)


def remote(src, dst, send_sem, recv_sem, target):
    return pltpu.make_async_remote_copy(
        src_ref=src,
        dst_ref=dst,
        send_sem=send_sem,
        recv_sem=recv_sem,
        device_id=target,
        device_id_type=MESH_ID,
    )


def greet(barrier, target):
    pl.semaphore_signal(barrier, inc=1, device_id=target, device_id_type=MESH_ID)


PIECES = 8
ROW_PIECES = 4


def aligned(start, size):
    return pl.ds(pl.multiple_of(start, size), size)


def layer_kernel(names, sp_count, score_scale, *refs):
    r = types.SimpleNamespace(**dict(zip(names, refs)))
    me, tp = lax.axis_index("sp"), lax.axis_index("tp")
    line = sp_count // 2
    last = line - 1
    z, y = me // 2, me % 2
    x, c = tp // 2, tp % 2
    mate_block = 2 * z + 1 - y
    mate = (mate_block, tp)
    above = (jnp.minimum(me + 2, sp_count - 1), tp)
    below = (jnp.maximum(me - 2, 0), tp)
    core_mate = (me, 2 * x + 1 - c)
    x_mate = (me, 2 * (1 - x) + c)
    not_last, not_first = z < last, z > 0
    q_rows = r.q_hbm.shape[0]
    rows, width = r.res_ref.shape
    f32, bf16 = jnp.float32, jnp.bfloat16

    barrier = pltpu.get_barrier_semaphore()
    for peer in (mate, core_mate, x_mate):
        greet(barrier, peer)

    @pl.when(not_last)
    def _():
        greet(barrier, above)

    @pl.when(not_first)
    def _():
        greet(barrier, below)

    def lanes(ref, head):
        return ref.at[:, aligned(head * HEAD_DIM, HEAD_DIM)]

    def q_part(ref, j):
        return ref.at[pl.ds(j * q_rows, q_rows), :]

    loads = [
        (lanes(r.k_hbm, 1 - y), r.ksend),
        (lanes(r.v_hbm, 1 - y), r.vsend),
        (lanes(r.k_hbm, y), r.kbuf.at[me]),
        (lanes(r.v_hbm, y), r.vbuf.at[me]),
        (lanes(r.q_hbm, 2 * (1 - y)), q_part(r.qsend, 0)),
        (lanes(r.q_hbm, 2 * (1 - y) + 1), q_part(r.qsend, 1)),
        (lanes(r.q_hbm, 2 * y), q_part(r.qs.at[y], 0)),
        (lanes(r.q_hbm, 2 * y + 1), q_part(r.qs.at[y], 1)),
    ]
    loads = [pltpu.make_async_copy(a, b, r.load_sem.at[i]) for i, (a, b) in enumerate(loads)]
    for copy in loads:
        copy.start()
    sources = (r.wo_hbm, r.eg_hbm, r.eu_hbm, r.ed_hbm, r.sg_hbm, r.su_hbm, r.sd_hbm)
    held = (r.wo, r.eg.at[0], r.eu.at[0], r.ed.at[0], r.sg, r.su, r.sd)
    weights = [pltpu.make_async_copy(a, b, r.weight_sem.at[i]) for i, (a, b) in enumerate(zip(sources, held))]
    first_f, second_f = r.f_ref[0:2, :], r.f_ref[2:4, :]
    r.fsend[...] = jnp.zeros(r.fsend.shape, f32)
    r.fbuf[me] = jnp.zeros(r.fsend.shape, f32)
    r.fsend[0:2, :] = jnp.where(y == 0, second_f, first_f)
    r.fbuf[me, 0:2, :] = jnp.where(y == 0, first_f, second_f)
    scores = r.score_ref[...]
    gates = scores / jnp.sum(scores, axis=0, keepdims=True) * routed_scale
    for e in range(sp_count):
        r.gbuf[z, e : e + 1, :] = jnp.sum(jnp.where(r.ids_ref[...] == e, gates, 0.0), axis=0, keepdims=True)
    r.acc[...] = jnp.zeros(r.acc.shape, f32)
    r.den[...] = jnp.zeros(r.den.shape, f32)
    r.top[...] = jnp.full(r.top.shape, -jnp.inf, f32)
    for copy in loads:
        copy.wait()
    pl.semaphore_wait(barrier, 3 + not_last.astype(jnp.int32) + not_first.astype(jnp.int32))

    def side_moves(block, sources):
        bufs = (r.fbuf, r.kbuf, r.vbuf)
        return [
            remote(a, b.at[block], r.side_send.at[i], r.kv_recv.at[block, i], mate)
            for i, (a, b) in enumerate(zip(sources, bufs))
        ]

    def up_moves(block, target):
        return [
            remote(b.at[block], b.at[block], r.kv_send.at[block, i], r.kv_recv.at[block, i], target)
            for i, b in enumerate((r.fbuf, r.kbuf, r.vbuf))
        ]

    def pass_up(block):
        @pl.when(not_last)
        def _():
            for copy in up_moves(block, above):
                copy.start()

    def q_move(slot):
        return remote(r.qsend, r.qs.at[slot], r.side_send.at[3], r.q_recv.at[0], mate)

    def parts(refs, quarter, i):
        g, u, d = refs
        tall, flat, wide = g.shape[0] // 4 // PIECES, d.shape[0] // 4, d.shape[1] // PIECES
        span = aligned((quarter * PIECES + i) * tall, tall)
        return (g.at[span, :], u.at[span, :], d.at[aligned(quarter * flat, flat), aligned(i * wide, wide)])

    own_expert = (r.eg_hbm, r.eu_hbm, r.ed_hbm)
    mates_expert = (r.eg.at[1], r.eu.at[1], r.ed.at[1])

    def w_moves(sources, quarter, i, send, recv, target):
        return [
            remote(a, b, send.at[i, k], recv.at[i, k], target)
            for k, (a, b) in enumerate(zip(parts(sources, quarter, i), parts(mates_expert, quarter, i)))
        ]

    def w_side(i):
        return w_moves(own_expert, tp, i, r.wy_send, r.wy_recv, mate)

    def w_hop(i, quarter):
        return w_moves(mates_expert, quarter, i, r.wx_send, r.wx_recv, x_mate)

    def w_core(part, i, quarter):
        return w_moves(mates_expert, quarter, i, r.wc_send.at[part], r.wc_recv.at[part], core_mate)

    x_quarter = 2 * (1 - x) + c

    def issue_weights(start, stop):
        def one(i, _):
            for copy in w_side(i):
                copy.start()
            return 0

        lax.fori_loop(start, stop, one, 0)

    def spread_x(i):
        for copy in w_hop(i, x_quarter):
            copy.wait_recv()
        for copy in w_core(1, i, x_quarter):
            copy.start()

    def spread(start, stop):
        def one(i, _):
            for copy in w_side(i):
                copy.wait_recv()
            for copy in w_hop(i, tp):
                copy.start()
            for copy in w_core(0, i, tp):
                copy.start()

            @pl.when(i >= 2)
            def _():
                spread_x(i - 2)

            return 0

        lax.fori_loop(start, stop, one, 0)

    def at_z(*values):
        out = values[-1]
        for level in range(len(values) - 1):
            out = jnp.where(z == level, values[level], out)
        return out

    early = jnp.maximum(2 * z - 1, 0)
    for copy in side_moves(me, (r.fsend, r.ksend, r.vsend)):
        copy.start()
    q_move(y).start()
    pass_up(me)
    issue_weights(0, early)
    for copy in weights:
        copy.start()

    def absorb(i, block, masked):
        q_block = 2 * z + i
        keys, values = r.kbuf[block], r.vbuf[block]
        for j in range(2):
            span = slice(j * q_rows, (j + 1) * q_rows)
            products = lax.dot_general(
                keys, r.qs[i, span, :], (((1,), (1,)), ((), ())), preferred_element_type=f32
            )
            column = jnp.broadcast_to(r.fbuf[block, j : j + 1, :], (HEAD_DIM, q_rows)).T
            column = jnp.concatenate([column] * (q_rows // HEAD_DIM), axis=1)
            drop = r.fbuf[q_block, j : j + 1, :] - column
            part = products * (score_scale * LOG2E) + drop * LOG2E
            if masked:
                at_key = lax.broadcasted_iota(jnp.int32, part.shape, 0)
                at_query = lax.broadcasted_iota(jnp.int32, part.shape, 1)
                part = jnp.where(at_query >= at_key, part, -jnp.inf)
            old = r.top[i, :1, span]
            peak = jnp.maximum(old, jnp.max(part, axis=0, keepdims=True))
            factor = jnp.exp2(old - peak)
            w = jnp.exp2(part - peak)
            r.den[i, :1, span] = r.den[i, :1, span] * factor + jnp.sum(w, axis=0, keepdims=True)
            mixed = lax.dot_general(
                values, w.astype(bf16), (((0,), (0,)), ((), ())), preferred_element_type=f32
            )
            r.acc[i, :, span] = r.acc[i, :, span] * factor + mixed
            r.top[i, :1, span] = peak

    absorb(y, me, True)
    for copy in side_moves(mate_block, (r.fsend, r.ksend, r.vsend)):
        copy.wait_recv()
    pass_up(mate_block)
    q_move(1 - y).wait_recv()
    absorb(1 - y, mate_block, True)
    absorb(1, 2 * z, False)

    def take(turn, _):
        level = z - 1 - turn // 2
        block = 2 * level + jnp.where(turn % 2 == 0, y, 1 - y)
        for copy in up_moves(block, below):
            copy.wait_recv()
        pass_up(block)
        absorb(1 - y, block, False)
        absorb(y, block, False)

        @pl.when(jnp.logical_and(z == last, jnp.logical_and(turn >= 3, turn < 5)))
        def _():
            spread(turn - 3, turn - 2)

        return 0

    lax.fori_loop(0, 2 * z, take, 0)

    def finish(i, target):
        for j in range(2):
            span = slice(j * q_rows, (j + 1) * q_rows)
            done = (r.acc[i, :, span] / r.den[i, :1, span]).T
            target[:, j * HEAD_DIM : (j + 1) * HEAD_DIM] = done.astype(bf16)

    def back_move(slot):
        return remote(r.attsend, r.att.at[slot], r.back_sem.at[0], r.back_sem.at[1], mate)

    finish(1 - y, r.attsend)
    back_move(y).start()
    issue_weights(early, PIECES)
    finish(y, r.att.at[y])
    marks = [at_z(0, 0, 0, 2), at_z(0, 1, 2, 3), at_z(0, 1, 3, 5), at_z(3, 3, 5, 7), at_z(5, 4, 6, 8)]
    marks += [at_z(8, 7, 8, 8), PIECES]
    spread(marks[0], marks[1])

    weights[0].wait()
    far, near = (1 - x) * 2, x * 2
    back_move(1 - y).wait_recv()
    half = r.att.shape[2]

    def core_copy(i):
        return remote(r.core_out.at[i], r.core_in.at[i], r.pair_sem.at[0, i], r.pair_sem.at[1, i], core_mate)

    part_rows = rows // ROW_PIECES

    def piece(ref, p):
        return ref.at[pl.ds(p * part_rows, part_rows), :]

    def hop(p):
        return remote(piece(r.x_out, p), piece(r.x_in, p), r.hop_sem.at[0, p], r.hop_sem.at[1, p], x_mate)

    def project_to(i, _):
        out_x = jnp.where(i == 0, far, near)
        span = aligned(out_x * rows, 2 * rows)
        r.pair[...] = jnp.dot(
            r.att[0, span, :], r.wo[0:half, :], preferred_element_type=f32
        ) + jnp.dot(r.att[1, span, :], r.wo[half : 2 * half, :], preferred_element_type=f32)
        r.core_out[i] = r.pair[aligned((1 - c) * rows, rows), :].astype(bf16)
        core_copy(i).start()
        r.kept[...] = r.pair[aligned(c * rows, rows), :]
        core_copy(i).wait_recv()

        @pl.when(i == 0)
        def _():
            for p in range(ROW_PIECES):
                span = slice(p * part_rows, (p + 1) * part_rows)
                r.x_out[span, :] = (r.kept[span, :] + r.core_in[0, span, :].astype(f32)).astype(bf16)
                hop(p).start()

        return 0

    lax.fori_loop(0, 2, project_to, 0)
    spread(marks[1], marks[2])

    def tok_move(level, p, send, target):
        return remote(
            piece(r.tok.at[level], p), piece(r.tok.at[level], p), send.at[level, p], r.tok_recv.at[level, p], target
        )

    def gate_move(level, send, target):
        return remote(r.gbuf.at[level], r.gbuf.at[level], send.at[level], r.gate_recv.at[level], target)

    @pl.when(not_last)
    def _():
        gate_move(z, r.gate_up, above).start()

    @pl.when(not_first)
    def _():
        gate_move(z, r.gate_dn, below).start()

    for p in range(ROW_PIECES):
        span = slice(p * part_rows, (p + 1) * part_rows)
        branch = r.kept[span, :] + r.core_in[1, span, :].astype(f32) + r.res_ref[span, :].astype(f32)
        hop(p).wait_recv()
        stream = (branch + r.x_in[span, :].astype(f32)).astype(bf16)
        wide = stream.astype(f32)
        scale = lax.rsqrt(jnp.mean(wide * wide, axis=1, keepdims=True) + norm_eps)
        r.tok[z, span, :] = (wide * scale * r.gain_ref[...]).astype(bf16)
        r.base[span, :] = wide

        @pl.when(not_last)
        def _():
            tok_move(z, p, r.tok_up, above).start()

        @pl.when(not_first)
        def _():
            tok_move(z, p, r.tok_dn, below).start()

    spread(marks[2], marks[3])
    for copy in weights[1:]:
        copy.wait()

    def gated(inputs, gate, up, down):
        first = jnp.dot(inputs, gate[...], preferred_element_type=f32)
        second = jnp.dot(inputs, up[...], preferred_element_type=f32)
        hidden = (first / (1.0 + jnp.exp(-first)) * second).astype(bf16)
        return jnp.dot(hidden, down[...], preferred_element_type=f32)

    def expert(level, slot, number):
        table = r.gbuf[level]
        at_expert = lax.broadcasted_iota(jnp.int32, table.shape, 0) == number
        row = jnp.sum(jnp.where(at_expert, table, 0.0), axis=0, keepdims=True)
        shape = (rows, row.shape[1])
        diagonal = lax.broadcasted_iota(jnp.int32, shape, 0) == lax.broadcasted_iota(jnp.int32, shape, 1)
        column = jnp.sum(jnp.where(diagonal, row, 0.0), axis=1, keepdims=True)
        result = gated(r.tok[level], r.eg.at[slot], r.eu.at[slot], r.ed.at[slot])
        return result.astype(bf16).astype(f32) * column

    def level_at(k):
        plain = k + (k >= z).astype(jnp.int32)
        swapped = jnp.where(k == last - 1, last - 2, jnp.where(k == last - 2, last, k))
        return jnp.where(z == last - 1, swapped, plain)

    def arrive(level):
        @pl.when(level < z)
        def _():
            gate_move(level, r.gate_up, below).wait_recv()

            @pl.when(not_last)
            def _():
                gate_move(level, r.gate_up, above).start()

            for p in range(ROW_PIECES):
                tok_move(level, p, r.tok_up, below).wait_recv()

                @pl.when(not_last)
                def _():
                    tok_move(level, p, r.tok_up, above).start()

        @pl.when(level > z)
        def _():
            gate_move(level, r.gate_dn, above).wait_recv()

            @pl.when(not_first)
            def _():
                gate_move(level, r.gate_dn, below).start()

            for p in range(ROW_PIECES):
                tok_move(level, p, r.tok_dn, above).wait_recv()

                @pl.when(not_first)
                def _():
                    tok_move(level, p, r.tok_dn, below).start()

    def up_back(level, p):
        return remote(
            piece(r.ret_out.at[level], p), piece(r.up_in.at[level], p), r.ret_send.at[level, p], r.up_recv.at[level, p], above
        )

    def dn_back(level, p):
        return remote(
            piece(r.ret_out.at[level], p), piece(r.dn_in.at[level], p), r.ret_send.at[level, p], r.dn_recv.at[level, p], below
        )

    def give_back(level):
        def send(back, came, chained):
            for p in range(ROW_PIECES):
                span = pl.ds(p * part_rows, part_rows)

                @pl.when(chained)
                def _():
                    back(level, p).wait_recv()
                    r.ret_out[level, span, :] = (
                        r.own[level, span, :] + came[level, span, :].astype(f32)
                    ).astype(bf16)

                @pl.when(jnp.logical_not(chained))
                def _():
                    r.ret_out[level, span, :] = r.own[level, span, :].astype(bf16)

                back(level, p).start()

        @pl.when(level > z)
        def _():
            send(up_back, r.up_in, not_first)

        @pl.when(level < z)
        def _():
            send(dn_back, r.dn_in, not_last)

    at_end = jnp.logical_or(z == 0, z == last)

    def first_turns(k, _):
        level = level_at(k)
        arrive(level)
        spread(jnp.where(k == 0, marks[3], marks[4]), jnp.where(k == 0, marks[4], marks[5]))
        r.own[level] = expert(level, 0, me)
        return 0

    lax.fori_loop(0, line - 2, first_turns, 0)
    spread(marks[5], PIECES)
    r.base[...] += gated(r.tok[z], r.sg, r.su, r.sd)
    spread_x(PIECES - 2)
    spread_x(PIECES - 1)

    def take_core(i, _):
        for copy in w_core(0, i, 2 * x + 1 - c) + w_core(1, i, 2 * (1 - x) + 1 - c):
            copy.wait_recv()
        return 0

    lax.fori_loop(0, PIECES, take_core, 0)

    @pl.when(z == last - 1)
    def _():
        arrive(level_at(line - 2))

    def second_turns(k, _):
        level = jnp.where(k < line - 1, level_at(k), z)

        @pl.when(k >= line - 2)
        def _():
            @pl.when(jnp.logical_and(k == line - 2, z != last - 1))
            def _():
                arrive(level)

            r.own[level] = expert(level, 0, me)

        r.own[level] += expert(level, 1, mate_block)

        @pl.when(jnp.logical_and(k < line - 1, at_end))
        def _():
            give_back(level)

        return 0

    lax.fori_loop(0, line, second_turns, 0)
    r.base[...] += r.own[z]

    def middle(k, _):
        @pl.when(jnp.logical_not(at_end))
        def _():
            order = jnp.where(
                z == last - 1,
                jnp.where(k < line - 2, k, last),
                jnp.where(k == 0, last - 1, jnp.where(k == 1, 0, last)),
            )
            give_back(order)

        return 0

    lax.fori_loop(0, line - 1, middle, 0)

    @pl.when(not_first)
    def _():
        for p in range(ROW_PIECES):
            up_back(z, p).wait_recv()
        r.base[...] += r.up_in[z].astype(f32)

    @pl.when(not_last)
    def _():
        for p in range(ROW_PIECES):
            dn_back(z, p).wait_recv()
        r.base[...] += r.dn_in[z].astype(f32)

    r.out_ref[...] = r.base[...].astype(bf16)

    for copy in side_moves(me, (r.fsend, r.ksend, r.vsend)) + [q_move(y), back_move(y)]:
        copy.wait_send()
    for i in range(2):
        core_copy(i).wait_send()
    for p in range(ROW_PIECES):
        hop(p).wait_send()

    def drain_weights(i, _):
        for copy in w_side(i) + w_hop(i, tp) + w_core(0, i, tp) + w_core(1, i, x_quarter):
            copy.wait_send()
        return 0

    lax.fori_loop(0, PIECES, drain_weights, 0)

    def drain(level, _):
        @pl.when(jnp.logical_and(level <= z, not_last))
        def _():
            for half_block in range(2):
                for copy in up_moves(2 * level + half_block, above):
                    copy.wait_send()
            gate_move(level, r.gate_up, above).wait_send()
            for p in range(ROW_PIECES):
                tok_move(level, p, r.tok_up, above).wait_send()

        @pl.when(jnp.logical_and(level >= z, not_first))
        def _():
            gate_move(level, r.gate_dn, below).wait_send()
            for p in range(ROW_PIECES):
                tok_move(level, p, r.tok_dn, below).wait_send()

        @pl.when(level > z)
        def _():
            for p in range(ROW_PIECES):
                up_back(level, p).wait_send()

        @pl.when(level < z)
        def _():
            for p in range(ROW_PIECES):
                dn_back(level, p).wait_send()

        return 0

    lax.fori_loop(0, line, drain, 0)


def layer_fused(
    residual,
    queries,
    key_rows,
    value_rows,
    forget_sums,
    norm_gain,
    expert_ids,
    route_weights,
    out_weight,
    expert_gate,
    expert_up,
    expert_down,
    shared_gate,
    shared_up,
    shared_down,
    sp_count,
):
    q_rows, features = queries.shape
    rows, width = residual.shape
    line = sp_count // 2
    bf16, f32 = jnp.bfloat16, jnp.float32
    vmem, hbm = pl.BlockSpec(memory_space=pltpu.VMEM), pl.BlockSpec(memory_space=pl.ANY)
    loaded = (
        out_weight,
        expert_gate[0],
        expert_up[0],
        expert_down[0],
        shared_gate,
        shared_up,
        shared_down,
    )
    ins = ["q_hbm", "f_ref", "k_hbm", "v_hbm", "res_ref", "gain_ref", "ids_ref", "score_ref"]
    ins += ["wo_hbm", "eg_hbm", "eu_hbm", "ed_hbm", "sg_hbm", "su_hbm", "sd_hbm"]
    one, per_level = (rows, width), (line, rows, width)
    stacked = (2 * q_rows, HEAD_DIM)

    def buf(*shape):
        return pltpu.VMEM(shape, bf16)

    def wide(*shape):
        return pltpu.VMEM(shape, f32)

    def dma(*shape):
        return pltpu.SemaphoreType.DMA(shape)

    scratch = {
        "qs": buf(2, *stacked),
        "qsend": buf(*stacked),
        "kbuf": buf(sp_count, q_rows, HEAD_DIM),
        "vbuf": buf(sp_count, q_rows, HEAD_DIM),
        "fbuf": wide(sp_count, 8, q_rows),
        "ksend": buf(q_rows, HEAD_DIM),
        "vsend": buf(q_rows, HEAD_DIM),
        "fsend": wide(8, q_rows),
        "acc": wide(2, HEAD_DIM, 2 * q_rows),
        "top": wide(2, 8, 2 * q_rows),
        "den": wide(2, 8, 2 * q_rows),
        "att": buf(2, q_rows, features // 2),
        "attsend": buf(q_rows, features // 2),
        "wo": buf(*out_weight.shape),
        "eg": buf(2, *expert_gate.shape[1:]),
        "eu": buf(2, *expert_up.shape[1:]),
        "ed": buf(2, *expert_down.shape[1:]),
        "sg": buf(*shared_gate.shape),
        "su": buf(*shared_up.shape),
        "sd": buf(*shared_down.shape),
        "gbuf": wide(line, sp_count, rows),
        "pair": wide(2 * rows, width),
        "kept": wide(*one),
        "core_out": buf(2, *one),
        "core_in": buf(2, *one),
        "x_out": buf(*one),
        "x_in": buf(*one),
        "base": wide(*one),
        "tok": buf(*per_level),
        "own": wide(*per_level),
        "ret_out": buf(*per_level),
        "up_in": buf(*per_level),
        "dn_in": buf(*per_level),
        "load_sem": dma(8),
        "weight_sem": dma(7),
        "side_send": dma(4),
        "q_recv": dma(1),
        "kv_send": dma(sp_count, 3),
        "kv_recv": dma(sp_count, 3),
        "back_sem": dma(2),
        "wy_send": dma(PIECES, 3),
        "wy_recv": dma(PIECES, 3),
        "wx_send": dma(PIECES, 3),
        "wx_recv": dma(PIECES, 3),
        "wc_send": dma(2, PIECES, 3),
        "wc_recv": dma(2, PIECES, 3),
        "pair_sem": dma(2, 2),
        "hop_sem": dma(2, ROW_PIECES),
        "tok_up": dma(line, ROW_PIECES),
        "tok_dn": dma(line, ROW_PIECES),
        "tok_recv": dma(line, ROW_PIECES),
        "gate_up": dma(line),
        "gate_dn": dma(line),
        "gate_recv": dma(line),
        "ret_send": dma(line, ROW_PIECES),
        "up_recv": dma(line, ROW_PIECES),
        "dn_recv": dma(line, ROW_PIECES),
    }
    names = ins + ["out_ref"] + list(scratch)
    return pl.pallas_call(
        functools.partial(layer_kernel, names, sp_count, HEAD_DIM ** (-0.5)),
        out_shape=jax.ShapeDtypeStruct(one, bf16),
        in_specs=[hbm, vmem, hbm, hbm] + [vmem] * 4 + [hbm] * 7,
        out_specs=vmem,
        scratch_shapes=list(scratch.values()),
        compiler_params=pltpu.CompilerParams(
            collective_id=0, has_side_effects=True, vmem_limit_bytes=60 * 2**20
        ),
    )(
        queries,
        forget_sums.T,
        key_rows,
        value_rows,
        residual,
        norm_gain[None, :],
        expert_ids.T,
        route_weights.T,
        *loaded,
    )


def absorb_group(carried, query_group, shard_piece, sum_piece, score_scale):
    query_heads, query_sums, query_pos, last_pos = query_group
    key_piece, value_piece = shard_piece
    piece_rows = key_piece.shape[0]
    query_count, local_kv, group_size, head_size = query_heads.shape
    key_block = math.gcd(piece_rows, 1024)
    key_heads = key_piece.reshape(piece_rows, local_kv, head_size)
    value_heads = value_piece.reshape(piece_rows, local_kv, head_size)
    key_sums = sum_piece.reshape(piece_rows, local_kv, group_size).transpose(1, 2, 0)

    def update(block_start, held):
        row_max, row_sum, weighted = held
        key_part = lax.dynamic_slice_in_dim(key_heads, block_start, key_block, 0)
        value_part = lax.dynamic_slice_in_dim(value_heads, block_start, key_block, 0)
        sums_part = lax.dynamic_slice_in_dim(key_sums, block_start, key_block, 2)
        scores = (
            jnp.einsum("qhgd,khd->hgqk", query_heads, key_part, preferred_element_type=jnp.float32)
            * score_scale
        )
        scores = scores + (query_sums[:, :, :, None] - sums_part[:, :, None, :])
        key_pos = block_start + jnp.arange(key_block, dtype=jnp.int32)
        allowed = query_pos[:, None] >= key_pos[None, :]
        scores = jnp.where(allowed, scores, -jnp.inf)
        new_max = jnp.maximum(row_max, jnp.max(scores, axis=3))
        weights = jnp.exp(scores - new_max[:, :, :, None])
        factor = jnp.exp(row_max - new_max)
        row_sum = row_sum * factor + jnp.sum(weights, axis=3)
        products = jnp.einsum(
            "hgqk,khd->qhgd",
            weights.astype(jnp.bfloat16),
            value_part,
            preferred_element_type=jnp.float32,
        )
        weighted = weighted * factor.transpose(2, 0, 1)[:, :, :, None] + products
        return (new_max, row_sum, weighted)

    def one_block(block_index, held):
        block_start = block_index * key_block
        needed = block_start <= last_pos
        return lax.cond(needed, lambda inner: update(block_start, inner), lambda inner: inner, held)

    return lax.fori_loop(0, piece_rows // key_block, one_block, carried)


def finish(carried):
    row_max, row_sum, weighted = carried
    mixed = weighted / row_sum.transpose(2, 0, 1)[:, :, :, None]
    return mixed.reshape(mixed.shape[0], -1).astype(jnp.bfloat16)


def local(
    residual,
    queries,
    key_rows,
    value_rows,
    forget_sums,
    out_weight,
    norm_gain,
    expert_ids,
    route_weights,
    expert_gate,
    expert_up,
    expert_down,
    shared_gate,
    shared_up,
    shared_down,
):
    sp_count = lax.axis_size("sp")
    sp_index = lax.axis_index("sp")
    local_rows = queries.shape[0]
    local_kv = key_rows.shape[1] // HEAD_DIM
    group_size = HEADS // KV_HEADS
    score_scale = HEAD_DIM ** (-0.5)
    tp_count = lax.axis_size("tp")
    tokens_here = residual.shape[0]
    every_slot = 2 * tokens_here * TOPK >= tokens_here * expert_gate.shape[0] * sp_count
    if every_slot and expert_gate.shape[0] == 1 and sp_count == 8 and tp_count == 4:
        return layer_fused(
            residual,
            queries,
            key_rows,
            value_rows,
            forget_sums,
            norm_gain,
            expert_ids,
            route_weights,
            out_weight,
            expert_gate,
            expert_up,
            expert_down,
            shared_gate,
            shared_up,
            shared_down,
            sp_count,
        )
    own_first = sp_index * local_rows
    all_sums = lax.all_gather(forget_sums, "sp", axis=0, tiled=True)
    positions = own_first + jnp.arange(local_rows, dtype=jnp.int32)
    groups = [
        (
            queries.reshape(queries.shape[0], local_kv, group_size, HEAD_DIM),
            forget_sums.reshape(forget_sums.shape[0], local_kv, group_size).transpose(1, 2, 0),
            positions,
            positions[-1],
        )
    ]

    def initial(query_count):
        return (
            jnp.full((local_kv, group_size, query_count), -1e30, jnp.float32),
            jnp.zeros((local_kv, group_size, query_count), jnp.float32),
            jnp.zeros((query_count, local_kv, group_size, HEAD_DIM), jnp.float32),
        )

    def absorb(states, shard_piece):
        return tuple(
            (
                absorb_group(held, query_group, shard_piece, all_sums, score_scale)
                for held, query_group in zip(states, groups)
            )
        )

    start_states = tuple((initial(query_group[0].shape[0]) for query_group in groups))
    states = absorb(
        start_states,
        (
            lax.all_gather(key_rows, "sp", axis=0, tiled=True),
            lax.all_gather(value_rows, "sp", axis=0, tiled=True),
        ),
    )
    outputs = [finish(held) for held in states]
    attended = outputs[0]
    rows_out = local_rows // lax.axis_size("tp")
    branch = lax.psum_scatter(
        jnp.dot(attended, out_weight, preferred_element_type=jnp.float32).astype(jnp.bfloat16),
        "tp",
        scatter_dimension=0,
        tiled=True,
    ).astype(jnp.float32)
    stream = (residual.astype(jnp.float32) + branch).astype(jnp.bfloat16)
    wide = lax.optimization_barrier(stream).astype(jnp.float32)
    normed = (
        wide * lax.rsqrt(jnp.mean(wide * wide, axis=1, keepdims=True) + norm_eps) * norm_gain
    ).astype(jnp.bfloat16)
    width = normed.shape[1]
    experts_here = expert_gate.shape[0]
    total_experts = experts_here * sp_count
    capacity = 2 * rows_out * TOPK // total_experts
    flat_ids = expert_ids.reshape(-1)
    assigned = flat_ids.shape[0]
    onehot = (flat_ids[:, None] == jnp.arange(total_experts, dtype=jnp.int32)[None, :]).astype(
        jnp.int32
    )
    slot_rank = jnp.sum((jnp.cumsum(onehot, axis=0) - 1) * onehot, axis=1)
    target = flat_ids * capacity + slot_rank
    slot_count = total_experts * capacity
    source = (
        jnp.full((slot_count,), assigned, jnp.int32)
        .at[target]
        .set(jnp.arange(assigned, dtype=jnp.int32))
    )
    padded = jnp.concatenate([normed, jnp.zeros((1, width), jnp.bfloat16)], axis=0)
    outgoing = padded[source // TOPK].reshape(sp_count, experts_here, capacity, width)
    arrived = lax.all_to_all(outgoing, "sp", split_axis=0, concat_axis=0, tiled=True)
    gate_part = jnp.einsum(
        "necd,edf->necf", arrived, expert_gate, preferred_element_type=jnp.float32
    )
    up_part = jnp.einsum("necd,edf->necf", arrived, expert_up, preferred_element_type=jnp.float32)
    hidden = (jax.nn.silu(gate_part) * up_part).astype(jnp.bfloat16)
    processed = jnp.einsum(
        "necf,efd->necd", hidden, expert_down, preferred_element_type=jnp.float32
    ).astype(jnp.bfloat16)
    returned = lax.all_to_all(processed, "sp", split_axis=0, concat_axis=0, tiled=True)
    results = returned.reshape(slot_count, width)
    picked = results[target].reshape(rows_out, TOPK, width).astype(jnp.float32)
    gates = route_weights / jnp.sum(route_weights, axis=1, keepdims=True) * routed_scale
    routed = jnp.sum(gates[:, :, None] * picked, axis=1)
    shared_hidden = (
        jax.nn.silu(jnp.dot(normed, shared_gate, preferred_element_type=jnp.float32))
        * jnp.dot(normed, shared_up, preferred_element_type=jnp.float32)
    ).astype(jnp.bfloat16)
    shared_out = jnp.dot(shared_hidden, shared_down, preferred_element_type=jnp.float32)
    return (wide + shared_out + routed).astype(jnp.bfloat16)


def solution(mesh):
    in_specs = (
        P(("sp", "tp"), None),
        P("sp", "tp"),
        P("sp", "tp"),
        P("sp", "tp"),
        P("sp", "tp"),
        P("tp", None),
        P(),
        P(("sp", "tp"), None),
        P(("sp", "tp"), None),
        P("sp", None, None),
        P("sp", None, None),
        P("sp", None, None),
        P(),
        P(),
        P(),
    )
    out_specs = P(("sp", "tp"), None)
    return jax.shard_map(local, mesh=mesh, in_specs=in_specs, out_specs=out_specs, check_vma=False)
```

time: 96.8 us -> 92.4 us (0.955)
  Pallas kernels: 94.9 us -> 90.6 us
    pallas_call x1, Pallas kernels: 94.9 us -> 90.6 us  [layer_fused(): pl.pallas_call(functools.partial(layer_kernel, names, sp_count, HEAD_DIM...]
where the time goes in v1:
time: 92.4 us; the launch traced here: 92.2 us
  Pallas kernels  90.6 us (98%)
  local copies, waits for them, and re-layouts  1.67 us (2%)
    pallas_call x1, Pallas kernels, layer_fused(): pl.pallas_call(functools.partial(layer_kernel, names, sp_count, HEAD_DIM...  90.6 us

profile of v1, /device:TPU:24, one launch (start us, length us, event | category | flops | bytes accessed | tf_op | source)
XLA Modules:
  0.0 92.2 jit_solution(6949102123362082368)
XLA Ops:
  0.0 90.6 %shard_map.145 = bf16[64,2048]{1,0:T(8,128)(2,1)} custom-call(bf16[256,512]{1,0:T(8,128)(2,1)} %refs_0_.1, f32[4,256]{1,0:T(4,128)} %bitcast.11, bf16[256,256]{1,0:T(8,128)(2,1)} %refs_2_.1, bf16[256,256]{1,0:T(8,128)(2,1)} %refs_3_.1, bf16[64,2048]{1,0:T(8,128)(2,1)} %refs_4_.1, f32[1,2048]{1,0:T(1,128)} %bitcast.10, s32[4,64]{1,0:T(4,128)} %bitcast.12, ...), custom_call_target="tpu_custom_call" | custom-call | tf_op jit(solution)/shard_map/pallas_call | solution.py:672
  90.6 1.7 %copy.17 = bf16[64,2048]{1,0:T(8,128)(2,1)} copy(bf16[64,2048]{1,0:T(8,128)(2,1)} %shard_map.145) | data formatting | bytes 524288

commit v2 on v1

--- a/solution.py
+++ b/solution.py
@@ -39,6 +39,7 @@
 
 
 PIECES = 8
+EXTRA = 1
 ROW_PIECES = 4
 
 
@@ -61,7 +62,7 @@
     x_mate = (me, 2 * (1 - x) + c)
     not_last, not_first = z < last, z > 0
     q_rows = r.q_hbm.shape[0]
-    rows, width = r.res_ref.shape
+    rows, width = r.res_hbm.shape
     f32, bf16 = jnp.float32, jnp.bfloat16
 
     barrier = pltpu.get_barrier_semaphore()
@@ -91,6 +92,11 @@
         (lanes(r.q_hbm, 2 * (1 - y) + 1), q_part(r.qsend, 1)),
         (lanes(r.q_hbm, 2 * y), q_part(r.qs.at[y], 0)),
         (lanes(r.q_hbm, 2 * y + 1), q_part(r.qs.at[y], 1)),
+        (r.f_hbm, r.f_ref),
+        (r.ids_hbm, r.ids_ref),
+        (r.score_hbm, r.score_ref),
+        (r.res_hbm, r.res_ref),
+        (r.gain_hbm, r.gain_ref),
     ]
     loads = [pltpu.make_async_copy(a, b, r.load_sem.at[i]) for i, (a, b) in enumerate(loads)]
     for copy in loads:
@@ -98,20 +104,16 @@
     sources = (r.wo_hbm, r.eg_hbm, r.eu_hbm, r.ed_hbm, r.sg_hbm, r.su_hbm, r.sd_hbm)
     held = (r.wo, r.eg.at[0], r.eu.at[0], r.ed.at[0], r.sg, r.su, r.sd)
     weights = [pltpu.make_async_copy(a, b, r.weight_sem.at[i]) for i, (a, b) in enumerate(zip(sources, held))]
-    first_f, second_f = r.f_ref[0:2, :], r.f_ref[2:4, :]
-    r.fsend[...] = jnp.zeros(r.fsend.shape, f32)
-    r.fbuf[me] = jnp.zeros(r.fsend.shape, f32)
-    r.fsend[0:2, :] = jnp.where(y == 0, second_f, first_f)
-    r.fbuf[me, 0:2, :] = jnp.where(y == 0, first_f, second_f)
-    scores = r.score_ref[...]
-    gates = scores / jnp.sum(scores, axis=0, keepdims=True) * routed_scale
-    for e in range(sp_count):
-        r.gbuf[z, e : e + 1, :] = jnp.sum(jnp.where(r.ids_ref[...] == e, gates, 0.0), axis=0, keepdims=True)
     r.acc[...] = jnp.zeros(r.acc.shape, f32)
     r.den[...] = jnp.zeros(r.den.shape, f32)
     r.top[...] = jnp.full(r.top.shape, -jnp.inf, f32)
-    for copy in loads:
+    r.fsend[...] = jnp.zeros(r.fsend.shape, f32)
+    r.fbuf[me] = jnp.zeros(r.fsend.shape, f32)
+    for copy in [loads[8]] + loads[:8]:
         copy.wait()
+    first_f, second_f = r.f_ref[0:2, :], r.f_ref[2:4, :]
+    r.fsend[0:2, :] = jnp.where(y == 0, second_f, first_f)
+    r.fbuf[me, 0:2, :] = jnp.where(y == 0, first_f, second_f)
     pl.semaphore_wait(barrier, 3 + not_last.astype(jnp.int32) + not_first.astype(jnp.int32))
 
     def side_moves(block, sources):
@@ -123,7 +125,7 @@
 
     def up_moves(block, target):
         return [
-            remote(b.at[block], b.at[block], r.kv_send.at[block, i], r.kv_recv.at[block, i], target)
+            remote(b.at[block], b.at[block], r.kv_send.at[i], r.kv_recv.at[block, i], target)
             for i, b in enumerate((r.fbuf, r.kbuf, r.vbuf))
         ]
 
@@ -142,53 +144,62 @@
         span = aligned((quarter * PIECES + i) * tall, tall)
         return (g.at[span, :], u.at[span, :], d.at[aligned(quarter * flat, flat), aligned(i * wide, wide)])
 
-    own_expert = (r.eg_hbm, r.eu_hbm, r.ed_hbm)
+    own_expert = (r.eg.at[0], r.eu.at[0], r.ed.at[0])
     mates_expert = (r.eg.at[1], r.eu.at[1], r.ed.at[1])
 
     def w_moves(sources, quarter, i, send, recv, target):
         return [
-            remote(a, b, send.at[i, k], recv.at[i, k], target)
-            for k, (a, b) in enumerate(zip(parts(sources, quarter, i), parts(mates_expert, quarter, i)))
+            remote(a, b, send, recv, target)
+            for a, b in zip(parts(sources, quarter, i), parts(mates_expert, quarter, i))
         ]
 
-    def w_side(i):
-        return w_moves(own_expert, tp, i, r.wy_send, r.wy_recv, mate)
-
-    def w_hop(i, quarter):
-        return w_moves(mates_expert, quarter, i, r.wx_send, r.wx_recv, x_mate)
-
-    def w_core(part, i, quarter):
-        return w_moves(mates_expert, quarter, i, r.wc_send.at[part], r.wc_recv.at[part], core_mate)
+    piece_rows = 3 * (r.eg.shape[1] // 4 // PIECES)
+
+    def w_all(count, send, recv, target):
+        one = r.eg.at[1, 0 : count * piece_rows, :]
+        return remote(one, one, send, recv, target)
+
+    def w_core_all():
+        both = r.eg.at[:, 0 : PIECES * piece_rows, :]
+        return remote(both, both, r.wc_sem.at[0], r.wc_sem.at[1], core_mate)
 
     x_quarter = 2 * (1 - x) + c
 
     def issue_weights(start, stop):
         def one(i, _):
-            for copy in w_side(i):
+            for copy in w_moves(own_expert, tp, i, r.wy_send.at[0], r.wy_recv.at[i], mate):
                 copy.start()
             return 0
 
         lax.fori_loop(start, stop, one, 0)
 
-    def spread_x(i):
-        for copy in w_hop(i, x_quarter):
-            copy.wait_recv()
-        for copy in w_core(1, i, x_quarter):
+    def issue_extra():
+        for i in range(PIECES - EXTRA, PIECES):
+            for copy in w_moves(own_expert, x_quarter, i, r.wy_send.at[0], r.wy_recv.at[EXTRA + i], mate):
+                copy.start()
+
+    def to_core(i, quarter):
+        for copy in w_moves(mates_expert, quarter, i, r.wc_sem.at[0], r.wc_sem.at[1], core_mate):
             copy.start()
 
     def spread(start, stop):
         def one(i, _):
-            for copy in w_side(i):
-                copy.wait_recv()
-            for copy in w_hop(i, tp):
-                copy.start()
-            for copy in w_core(0, i, tp):
-                copy.start()
-
-            @pl.when(i >= 2)
+            w_all(1, r.wy_send.at[0], r.wy_recv.at[i], mate).wait_recv()
+
+            @pl.when(i < PIECES - EXTRA)
             def _():
-                spread_x(i - 2)
-
+                for copy in w_moves(mates_expert, tp, i, r.wx_send.at[0], r.wx_recv.at[i], x_mate):
+                    copy.start()
+
+            to_core(i, tp)
+            return 0
+
+        lax.fori_loop(start, stop, one, 0)
+
+    def spread_x(start, stop):
+        def one(i, _):
+            w_all(1, r.wx_send.at[0], r.wx_recv.at[i], x_mate).wait_recv()
+            to_core(i, x_quarter)
             return 0
 
         lax.fori_loop(start, stop, one, 0)
@@ -199,14 +210,18 @@
             out = jnp.where(z == level, values[level], out)
         return out
 
-    early = jnp.maximum(2 * z - 1, 0)
+    early = at_z(1, 1, 4, 5)
     for copy in side_moves(me, (r.fsend, r.ksend, r.vsend)):
         copy.start()
-    q_move(y).start()
     pass_up(me)
-    issue_weights(0, early)
-    for copy in weights:
+    for copy in weights[1:4]:
         copy.start()
+    for copy in loads[9:]:
+        copy.wait()
+    scores = r.score_ref[...]
+    gates = scores / jnp.sum(scores, axis=0, keepdims=True) * routed_scale
+    for e in range(sp_count):
+        r.gbuf[z, e : e + 1, :] = jnp.sum(jnp.where(r.ids_ref[...] == e, gates, 0.0), axis=0, keepdims=True)
 
     def absorb(i, block, masked):
         q_block = 2 * z + i
@@ -236,25 +251,66 @@
             r.top[i, :1, span] = peak
 
     absorb(y, me, True)
+    q_move(y).start()
+    for copy in weights[1:4]:
+        copy.wait()
+    issue_weights(0, early)
+    for copy in weights[:1] + weights[4:]:
+        copy.start()
+    def pick(turn, values):
+        out = values[-1]
+        for k in range(len(values) - 1):
+            out = jnp.where(turn == k, values[k], out)
+        return out
+
+    def turn_block(turn):
+        level = at_z(0, 0, pick(turn, (1, 0, 1, 0)), pick(turn, (2, 1, 2, 0, 1, 0)))
+        other = at_z(0, pick(turn, (0, 1)), pick(turn, (0, 0, 1, 1)), pick(turn, (0, 0, 1, 0, 1, 1)))
+        return 2 * level + jnp.where(other == 0, y, 1 - y)
+
+    def take_keys(turn):
+        block = turn_block(turn)
+        for copy in up_moves(block, below):
+            copy.wait_recv()
+        pass_up(block)
+
+    @pl.when(not_first)
+    def _():
+        take_keys(0)
+
     for copy in side_moves(mate_block, (r.fsend, r.ksend, r.vsend)):
         copy.wait_recv()
     pass_up(mate_block)
+
+    @pl.when(not_first)
+    def _():
+        take_keys(1)
+
     q_move(1 - y).wait_recv()
     absorb(1 - y, mate_block, True)
     absorb(1, 2 * z, False)
 
     def take(turn, _):
-        level = z - 1 - turn // 2
-        block = 2 * level + jnp.where(turn % 2 == 0, y, 1 - y)
-        for copy in up_moves(block, below):
-            copy.wait_recv()
-        pass_up(block)
+        ahead = jnp.where(z == last, turn, turn + 1)
+
+        @pl.when(jnp.logical_and(ahead >= 2, ahead < 2 * z))
+        def _():
+            take_keys(ahead)
+
+        block = turn_block(turn)
         absorb(1 - y, block, False)
-        absorb(y, block, False)
-
-        @pl.when(jnp.logical_and(z == last, jnp.logical_and(turn >= 3, turn < 5)))
-        def _():
-            spread(turn - 3, turn - 2)
+
+        @pl.when(turn < 2 * z - 1)
+        def _():
+            absorb(y, block, False)
+
+        @pl.when(jnp.logical_and(z == last, jnp.logical_and(turn >= 1, turn < 4)))
+        def _():
+            spread(turn - 1, turn)
+
+        @pl.when(jnp.logical_and(z == last - 1, jnp.logical_and(turn >= 1, turn < 3)))
+        def _():
+            spread(turn - 1, turn)
 
         return 0
 
@@ -266,20 +322,28 @@
             done = (r.acc[i, :, span] / r.den[i, :1, span]).T
             target[:, j * HEAD_DIM : (j + 1) * HEAD_DIM] = done.astype(bf16)
 
-    def back_move(slot):
-        return remote(r.attsend, r.att.at[slot], r.back_sem.at[0], r.back_sem.at[1], mate)
+    far, near = (1 - x) * 2, x * 2
+
+    def back_move(slot, i):
+        span = aligned((far if i == 0 else near) * rows, 2 * rows)
+        return remote(r.attsend.at[span, :], r.att.at[slot, span, :], r.back_send.at[i], r.back_recv.at[i], mate)
 
     finish(1 - y, r.attsend)
-    back_move(y).start()
+    for i in range(2):
+        back_move(y, i).start()
     issue_weights(early, PIECES)
+    issue_extra()
+
+    @pl.when(not_first)
+    def _():
+        absorb(y, 1 - y, False)
+
     finish(y, r.att.at[y])
-    marks = [at_z(0, 0, 0, 2), at_z(0, 1, 2, 3), at_z(0, 1, 3, 5), at_z(3, 3, 5, 7), at_z(5, 4, 6, 8)]
-    marks += [at_z(8, 7, 8, 8), PIECES]
+    marks = [at_z(0, 0, 2, 3), at_z(1, 1, 3, 4), at_z(2, 2, 5, 6), at_z(4, 4, 6, 8), at_z(6, 6, 7, 8)]
+    x_mark = at_z(1, 1, 3, 4)
     spread(marks[0], marks[1])
 
     weights[0].wait()
-    far, near = (1 - x) * 2, x * 2
-    back_move(1 - y).wait_recv()
     half = r.att.shape[2]
 
     def core_copy(i):
@@ -291,38 +355,39 @@
         return ref.at[pl.ds(p * part_rows, part_rows), :]
 
     def hop(p):
-        return remote(piece(r.x_out, p), piece(r.x_in, p), r.hop_sem.at[0, p], r.hop_sem.at[1, p], x_mate)
+        return remote(piece(r.x_out, p), piece(r.x_in, p), r.hop_send.at[0], r.hop_recv.at[p], x_mate)
 
     def project_to(i, _):
         out_x = jnp.where(i == 0, far, near)
+        back = remote(
+            r.attsend.at[0 : 2 * rows, :], r.attsend.at[0 : 2 * rows, :], r.back_send.at[i], r.back_recv.at[i], mate
+        )
+        back.wait_recv()
         span = aligned(out_x * rows, 2 * rows)
         r.pair[...] = jnp.dot(
             r.att[0, span, :], r.wo[0:half, :], preferred_element_type=f32
         ) + jnp.dot(r.att[1, span, :], r.wo[half : 2 * half, :], preferred_element_type=f32)
         r.core_out[i] = r.pair[aligned((1 - c) * rows, rows), :].astype(bf16)
         core_copy(i).start()
-        r.kept[...] = r.pair[aligned(c * rows, rows), :]
-        core_copy(i).wait_recv()
-
-        @pl.when(i == 0)
-        def _():
-            for p in range(ROW_PIECES):
-                span = slice(p * part_rows, (p + 1) * part_rows)
-                r.x_out[span, :] = (r.kept[span, :] + r.core_in[0, span, :].astype(f32)).astype(bf16)
-                hop(p).start()
-
+        r.kept[i] = r.pair[aligned(c * rows, rows), :]
         return 0
 
     lax.fori_loop(0, 2, project_to, 0)
+    core_copy(0).wait_recv()
+    for p in range(ROW_PIECES):
+        span = slice(p * part_rows, (p + 1) * part_rows)
+        r.x_out[span, :] = (r.kept[0, span, :] + r.core_in[0, span, :].astype(f32)).astype(bf16)
+        hop(p).start()
+    core_copy(1).wait_recv()
     spread(marks[1], marks[2])
 
     def tok_move(level, p, send, target):
         return remote(
-            piece(r.tok.at[level], p), piece(r.tok.at[level], p), send.at[level, p], r.tok_recv.at[level, p], target
+            piece(r.tok.at[level], p), piece(r.tok.at[level], p), send.at[0], r.tok_recv.at[level, p], target
         )
 
     def gate_move(level, send, target):
-        return remote(r.gbuf.at[level], r.gbuf.at[level], send.at[level], r.gate_recv.at[level], target)
+        return remote(r.gbuf.at[level], r.gbuf.at[level], send.at[0], r.gate_recv.at[level], target)
 
     @pl.when(not_last)
     def _():
@@ -334,7 +399,7 @@
 
     for p in range(ROW_PIECES):
         span = slice(p * part_rows, (p + 1) * part_rows)
-        branch = r.kept[span, :] + r.core_in[1, span, :].astype(f32) + r.res_ref[span, :].astype(f32)
+        branch = r.kept[1, span, :] + r.core_in[1, span, :].astype(f32) + r.res_ref[span, :].astype(f32)
         hop(p).wait_recv()
         stream = (branch + r.x_in[span, :].astype(f32)).astype(bf16)
         wide = stream.astype(f32)
@@ -351,7 +416,8 @@
             tok_move(z, p, r.tok_dn, below).start()
 
     spread(marks[2], marks[3])
-    for copy in weights[1:]:
+    spread_x(0, x_mark)
+    for copy in weights[4:]:
         copy.wait()
 
     def gated(inputs, gate, up, down):
@@ -370,50 +436,43 @@
         result = gated(r.tok[level], r.eg.at[slot], r.eu.at[slot], r.ed.at[slot])
         return result.astype(bf16).astype(f32) * column
 
-    def level_at(k):
-        plain = k + (k >= z).astype(jnp.int32)
-        swapped = jnp.where(k == last - 1, last - 2, jnp.where(k == last - 2, last, k))
-        return jnp.where(z == last - 1, swapped, plain)
-
-    def arrive(level):
+    def arrive_piece(level, p):
         @pl.when(level < z)
         def _():
-            gate_move(level, r.gate_up, below).wait_recv()
+            if p == 0:
+                gate_move(level, r.gate_up, below).wait_recv()
+            tok_move(level, p, r.tok_up, below).wait_recv()
 
             @pl.when(not_last)
             def _():
-                gate_move(level, r.gate_up, above).start()
-
-            for p in range(ROW_PIECES):
-                tok_move(level, p, r.tok_up, below).wait_recv()
-
-                @pl.when(not_last)
-                def _():
-                    tok_move(level, p, r.tok_up, above).start()
+                if p == 0:
+                    gate_move(level, r.gate_up, above).start()
+                tok_move(level, p, r.tok_up, above).start()
 
         @pl.when(level > z)
         def _():
-            gate_move(level, r.gate_dn, above).wait_recv()
+            if p == 0:
+                gate_move(level, r.gate_dn, above).wait_recv()
+            tok_move(level, p, r.tok_dn, above).wait_recv()
 
             @pl.when(not_first)
             def _():
-                gate_move(level, r.gate_dn, below).start()
-
-            for p in range(ROW_PIECES):
-                tok_move(level, p, r.tok_dn, above).wait_recv()
-
-                @pl.when(not_first)
-                def _():
-                    tok_move(level, p, r.tok_dn, below).start()
+                if p == 0:
+                    gate_move(level, r.gate_dn, below).start()
+                tok_move(level, p, r.tok_dn, below).start()
+
+    def arrive(level):
+        for p in range(ROW_PIECES):
+            arrive_piece(level, p)
 
     def up_back(level, p):
         return remote(
-            piece(r.ret_out.at[level], p), piece(r.up_in.at[level], p), r.ret_send.at[level, p], r.up_recv.at[level, p], above
+            piece(r.ret_out.at[level], p), piece(r.up_in.at[level], p), r.ret_send.at[0], r.up_recv.at[level, p], above
         )
 
     def dn_back(level, p):
         return remote(
-            piece(r.ret_out.at[level], p), piece(r.dn_in.at[level], p), r.ret_send.at[level, p], r.dn_recv.at[level, p], below
+            piece(r.ret_out.at[level], p), piece(r.dn_in.at[level], p), r.ret_send.at[0], r.dn_recv.at[level, p], below
         )
 
     def give_back(level):
@@ -442,67 +501,79 @@
         def _():
             send(dn_back, r.dn_in, not_last)
 
-    at_end = jnp.logical_or(z == 0, z == last)
+    def own_expert_on(level):
+        r.own[level] = expert(level, 0, me)
+
+    def mates_expert_on(level):
+        r.own[level] += expert(level, 1, mate_block)
 
     def first_turns(k, _):
-        level = level_at(k)
-        arrive(level)
-        spread(jnp.where(k == 0, marks[3], marks[4]), jnp.where(k == 0, marks[4], marks[5]))
-        r.own[level] = expert(level, 0, me)
+        level = jnp.where(k == 0, at_z(1, 0, 1, 2), jnp.where(k == 1, at_z(2, 2, 0, 1), z))
+
+        @pl.when(k < 2)
+        def _():
+            for p in range(ROW_PIECES):
+                arrive_piece(level, p)
+
+                @pl.when(jnp.logical_and(z == last - 1, k == 1))
+                def _():
+                    arrive_piece(last, p)
+
+            spread(jnp.where(k == 0, marks[3], marks[4]), jnp.where(k == 0, marks[4], PIECES))
+
+        own_expert_on(level)
         return 0
 
-    lax.fori_loop(0, line - 2, first_turns, 0)
-    spread(marks[5], PIECES)
+    lax.fori_loop(0, 3, first_turns, 0)
     r.base[...] += gated(r.tok[z], r.sg, r.su, r.sd)
-    spread_x(PIECES - 2)
-    spread_x(PIECES - 1)
-
-    def take_core(i, _):
-        for copy in w_core(0, i, 2 * x + 1 - c) + w_core(1, i, 2 * (1 - x) + 1 - c):
-            copy.wait_recv()
-        return 0
-
-    lax.fori_loop(0, PIECES, take_core, 0)
-
-    @pl.when(z == last - 1)
-    def _():
-        arrive(level_at(line - 2))
+
+    @pl.when(not_first)
+    def _():
+        level = at_z(0, 3, 3, 0)
+
+        @pl.when(z != last - 1)
+        def _():
+            arrive(level)
+
+        own_expert_on(level)
+
+    spread_x(x_mark, PIECES - EXTRA)
+    for i in range(PIECES - EXTRA, PIECES):
+        w_all(1, r.wy_send.at[0], r.wy_recv.at[EXTRA + i], mate).wait_recv()
+        to_core(i, x_quarter)
+    w_core_all().wait_recv()
 
     def second_turns(k, _):
-        level = jnp.where(k < line - 1, level_at(k), z)
-
-        @pl.when(k >= line - 2)
-        def _():
-            @pl.when(jnp.logical_and(k == line - 2, z != last - 1))
-            def _():
-                arrive(level)
-
-            r.own[level] = expert(level, 0, me)
-
-        r.own[level] += expert(level, 1, mate_block)
-
-        @pl.when(jnp.logical_and(k < line - 1, at_end))
+        level = jnp.where(k == line - 1, z, at_z(k + 1, pick(k, (3, 0, 2)), pick(k, (0, 3, 1)), k))
+
+        @pl.when(jnp.logical_and(z == 0, k == 2))
+        def _():
+            arrive(level)
+            own_expert_on(level)
+
+        mates_expert_on(level)
+
+        @pl.when(jnp.logical_or(jnp.logical_and(z == last, k < line - 1), jnp.logical_and(z == 0, k == 0)))
         def _():
             give_back(level)
+
+        @pl.when(jnp.logical_and(z == 0, k == 2))
+        def _():
+            give_back(last)
+            give_back(2)
 
         return 0
 
     lax.fori_loop(0, line, second_turns, 0)
     r.base[...] += r.own[z]
 
-    def middle(k, _):
-        @pl.when(jnp.logical_not(at_end))
-        def _():
-            order = jnp.where(
-                z == last - 1,
-                jnp.where(k < line - 2, k, last),
-                jnp.where(k == 0, last - 1, jnp.where(k == 1, 0, last)),
-            )
-            give_back(order)
-
-        return 0
-
-    lax.fori_loop(0, line - 1, middle, 0)
+    @pl.when(jnp.logical_and(not_first, not_last))
+    def _():
+        def middle(k, _):
+            give_back(at_z(0, pick(k, (3, 0, 2)), pick(k, (0, 3, 1)), 0))
+            return 0
+
+        lax.fori_loop(0, line - 1, middle, 0)
 
     @pl.when(not_first)
     def _():
@@ -518,49 +589,42 @@
 
     r.out_ref[...] = r.base[...].astype(bf16)
 
-    for copy in side_moves(me, (r.fsend, r.ksend, r.vsend)) + [q_move(y), back_move(y)]:
+    for copy in side_moves(me, (r.fsend, r.ksend, r.vsend)) + [q_move(y), back_move(y, 0), back_move(y, 1)]:
         copy.wait_send()
     for i in range(2):
         core_copy(i).wait_send()
-    for p in range(ROW_PIECES):
-        hop(p).wait_send()
-
-    def drain_weights(i, _):
-        for copy in w_side(i) + w_hop(i, tp) + w_core(0, i, tp) + w_core(1, i, x_quarter):
-            copy.wait_send()
-        return 0
-
-    lax.fori_loop(0, PIECES, drain_weights, 0)
-
-    def drain(level, _):
-        @pl.when(jnp.logical_and(level <= z, not_last))
-        def _():
-            for half_block in range(2):
-                for copy in up_moves(2 * level + half_block, above):
-                    copy.wait_send()
-            gate_move(level, r.gate_up, above).wait_send()
-            for p in range(ROW_PIECES):
-                tok_move(level, p, r.tok_up, above).wait_send()
-
-        @pl.when(jnp.logical_and(level >= z, not_first))
-        def _():
-            gate_move(level, r.gate_dn, below).wait_send()
-            for p in range(ROW_PIECES):
-                tok_move(level, p, r.tok_dn, below).wait_send()
-
-        @pl.when(level > z)
-        def _():
-            for p in range(ROW_PIECES):
-                up_back(level, p).wait_send()
-
-        @pl.when(level < z)
-        def _():
-            for p in range(ROW_PIECES):
-                dn_back(level, p).wait_send()
-
-        return 0
-
-    lax.fori_loop(0, line, drain, 0)
+    def sent(whole, send, recv, target):
+        remote(whole, whole, send, recv, target).wait_send()
+
+    sent(r.x_out, r.hop_send.at[0], r.hop_recv.at[0], x_mate)
+    w_all(PIECES + EXTRA, r.wy_send.at[0], r.wy_recv.at[0], mate).wait_send()
+    w_all(PIECES - EXTRA, r.wx_send.at[0], r.wx_recv.at[0], x_mate).wait_send()
+    w_core_all().wait_send()
+    done = pl.ds(0, line - 1)
+
+    @pl.when(not_last)
+    def _():
+        for level in range(last):
+
+            @pl.when(z == level)
+            def _():
+                blocks, levels = pl.ds(0, 2 * level + 2), pl.ds(0, level + 1)
+                for i, b in enumerate((r.fbuf, r.kbuf, r.vbuf)):
+                    sent(b.at[blocks], r.kv_send.at[i], r.kv_recv.at[0, i], above)
+                sent(r.gbuf.at[levels], r.gate_up.at[0], r.gate_recv.at[0], above)
+                sent(r.tok.at[levels], r.tok_up.at[0], r.tok_recv.at[0, 0], above)
+
+    @pl.when(not_first)
+    def _():
+        for level in range(1, line):
+
+            @pl.when(z == level)
+            def _():
+                levels = pl.ds(0, line - level)
+                sent(r.gbuf.at[levels], r.gate_dn.at[0], r.gate_recv.at[0], below)
+                sent(r.tok.at[levels], r.tok_dn.at[0], r.tok_recv.at[0, 0], below)
+
+    sent(r.ret_out.at[done], r.ret_send.at[0], r.up_recv.at[0, 0], above)
 
 
 def layer_fused(
@@ -595,7 +659,7 @@
         shared_up,
         shared_down,
     )
-    ins = ["q_hbm", "f_ref", "k_hbm", "v_hbm", "res_ref", "gain_ref", "ids_ref", "score_ref"]
+    ins = ["q_hbm", "f_hbm", "k_hbm", "v_hbm", "res_hbm", "gain_hbm", "ids_hbm", "score_hbm"]
     ins += ["wo_hbm", "eg_hbm", "eu_hbm", "ed_hbm", "sg_hbm", "su_hbm", "sd_hbm"]
     one, per_level = (rows, width), (line, rows, width)
     stacked = (2 * q_rows, HEAD_DIM)
@@ -632,7 +696,7 @@
         "sd": buf(*shared_down.shape),
         "gbuf": wide(line, sp_count, rows),
         "pair": wide(2 * rows, width),
-        "kept": wide(*one),
+        "kept": wide(2, *one),
         "core_out": buf(2, *one),
         "core_in": buf(2, *one),
         "x_out": buf(*one),
@@ -643,28 +707,34 @@
         "ret_out": buf(*per_level),
         "up_in": buf(*per_level),
         "dn_in": buf(*per_level),
-        "load_sem": dma(8),
+        "f_ref": wide(*forget_sums.shape[::-1]),
+        "res_ref": buf(*one),
+        "gain_ref": wide(1, width),
+        "ids_ref": pltpu.VMEM(expert_ids.shape[::-1], jnp.int32),
+        "score_ref": wide(*route_weights.shape[::-1]),
+        "load_sem": dma(13),
         "weight_sem": dma(7),
         "side_send": dma(4),
         "q_recv": dma(1),
-        "kv_send": dma(sp_count, 3),
+        "kv_send": dma(3),
         "kv_recv": dma(sp_count, 3),
-        "back_sem": dma(2),
-        "wy_send": dma(PIECES, 3),
-        "wy_recv": dma(PIECES, 3),
-        "wx_send": dma(PIECES, 3),
-        "wx_recv": dma(PIECES, 3),
-        "wc_send": dma(2, PIECES, 3),
-        "wc_recv": dma(2, PIECES, 3),
+        "back_send": dma(2),
+        "back_recv": dma(2),
+        "wy_send": dma(1),
+        "wy_recv": dma(PIECES + EXTRA),
+        "wx_send": dma(1),
+        "wx_recv": dma(PIECES),
+        "wc_sem": dma(2),
         "pair_sem": dma(2, 2),
-        "hop_sem": dma(2, ROW_PIECES),
-        "tok_up": dma(line, ROW_PIECES),
-        "tok_dn": dma(line, ROW_PIECES),
+        "hop_send": dma(1),
+        "hop_recv": dma(ROW_PIECES),
+        "tok_up": dma(1),
+        "tok_dn": dma(1),
         "tok_recv": dma(line, ROW_PIECES),
-        "gate_up": dma(line),
-        "gate_dn": dma(line),
+        "gate_up": dma(1),
+        "gate_dn": dma(1),
         "gate_recv": dma(line),
-        "ret_send": dma(line, ROW_PIECES),
+        "ret_send": dma(1),
         "up_recv": dma(line, ROW_PIECES),
         "dn_recv": dma(line, ROW_PIECES),
     }
@@ -672,7 +742,7 @@
     return pl.pallas_call(
         functools.partial(layer_kernel, names, sp_count, HEAD_DIM ** (-0.5)),
         out_shape=jax.ShapeDtypeStruct(one, bf16),
-        in_specs=[hbm, vmem, hbm, hbm] + [vmem] * 4 + [hbm] * 7,
+        in_specs=[hbm] * 15,
         out_specs=vmem,
         scratch_shapes=list(scratch.values()),
         compiler_params=pltpu.CompilerParams(

time: 92.4 us -> 77.4 us (0.84)
  the two profiles are of different devices: /device:TPU:24 before, /device:TPU:9 now
where the time goes in v2:
time: 77.4 us; the launch traced here: 77.3 us
  Pallas kernels  75.6 us (98%)
  local copies, waits for them, and re-layouts  1.67 us (2%)
    pallas_call x1, Pallas kernels, layer_fused(): pl.pallas_call(functools.partial(layer_kernel, names, sp_count, HEAD_DIM...  75.6 us
    unnamed x1, local copies, waits for them, and re-layouts  1.67 us

profile of v2, /device:TPU:9, one launch (start us, length us, event | category | flops | bytes accessed | tf_op | source)
XLA Modules:
  0.0 77.3 jit_solution(6117699263672922547)
XLA Ops:
  0.0 75.6 %shard_map.145 = bf16[64,2048]{1,0:T(8,128)(2,1)} custom-call(bf16[256,512]{1,0:T(8,128)(2,1)} %refs_0_.1, f32[4,256]{1,0:T(4,128)} %bitcast.11, bf16[256,256]{1,0:T(8,128)(2,1)} %refs_2_.1, bf16[256,256]{1,0:T(8,128)(2,1)} %refs_3_.1, bf16[64,2048]{1,0:T(8,128)(2,1)} %refs_4_.1, f32[1,2048]{1,0:T(1,128)} %bitcast.10, s32[4,64]{1,0:T(4,128)} %bitcast.12, ...), custom_call_target="tpu_custom_call" | custom-call | tf_op jit(solution)/shard_map/pallas_call | solution.py:742
  75.6 1.7 %copy.17 = bf16[64,2048]{1,0:T(8,128)(2,1)} copy(bf16[64,2048]{1,0:T(8,128)(2,1)} %shard_map.145) | data formatting | bytes 524288

commit v3 on v2

--- a/solution.py
+++ b/solution.py
@@ -210,7 +210,7 @@
             out = jnp.where(z == level, values[level], out)
         return out
 
-    early = at_z(1, 1, 4, 5)
+    early = at_z(1, 2, 3, 5)
     for copy in side_moves(me, (r.fsend, r.ksend, r.vsend)):
         copy.start()
     pass_up(me)
@@ -304,13 +304,17 @@
         def _():
             absorb(y, block, False)
 
-        @pl.when(jnp.logical_and(z == last, jnp.logical_and(turn >= 1, turn < 4)))
-        def _():
-            spread(turn - 1, turn)
-
-        @pl.when(jnp.logical_and(z == last - 1, jnp.logical_and(turn >= 1, turn < 3)))
-        def _():
-            spread(turn - 1, turn)
+        @pl.when(turn == 0)
+        def _():
+            spread(0, 1)
+
+        @pl.when(jnp.logical_and(z >= last - 1, turn == 2))
+        def _():
+            spread(1, 2)
+
+        @pl.when(jnp.logical_and(z == last, turn == 3))
+        def _():
+            spread(2, 3)
 
         return 0
 
@@ -339,8 +343,8 @@
         absorb(y, 1 - y, False)
 
     finish(y, r.att.at[y])
-    marks = [at_z(0, 0, 2, 3), at_z(1, 1, 3, 4), at_z(2, 2, 5, 6), at_z(4, 4, 6, 8), at_z(6, 6, 7, 8)]
-    x_mark = at_z(1, 1, 3, 4)
+    marks = [at_z(0, 1, 2, 3), at_z(1, 2, 3, 5), at_z(2, 3, 4, 6), at_z(6, 4, 6, 7), at_z(8, 6, 7, 8), at_z(8, 7, 8, 8)]
+    x_mark = at_z(1, 2, 3, 4)
     spread(marks[0], marks[1])
 
     weights[0].wait()
@@ -389,6 +393,35 @@
     def gate_move(level, send, target):
         return remote(r.gbuf.at[level], r.gbuf.at[level], send.at[0], r.gate_recv.at[level], target)
 
+    def arrive_piece(level, p):
+        @pl.when(level < z)
+        def _():
+            if p == 0:
+                gate_move(level, r.gate_up, below).wait_recv()
+            tok_move(level, p, r.tok_up, below).wait_recv()
+
+            @pl.when(not_last)
+            def _():
+                if p == 0:
+                    gate_move(level, r.gate_up, above).start()
+                tok_move(level, p, r.tok_up, above).start()
+
+        @pl.when(level > z)
+        def _():
+            if p == 0:
+                gate_move(level, r.gate_dn, above).wait_recv()
+            tok_move(level, p, r.tok_dn, above).wait_recv()
+
+            @pl.when(not_first)
+            def _():
+                if p == 0:
+                    gate_move(level, r.gate_dn, below).start()
+                tok_move(level, p, r.tok_dn, below).start()
+
+    def arrive(level):
+        for p in range(ROW_PIECES):
+            arrive_piece(level, p)
+
     @pl.when(not_last)
     def _():
         gate_move(z, r.gate_up, above).start()
@@ -407,6 +440,10 @@
         r.tok[z, span, :] = (wide * scale * r.gain_ref[...]).astype(bf16)
         r.base[span, :] = wide
 
+        @pl.when(z == 1)
+        def _():
+            arrive_piece(0, p)
+
         @pl.when(not_last)
         def _():
             tok_move(z, p, r.tok_up, above).start()
@@ -436,35 +473,6 @@
         result = gated(r.tok[level], r.eg.at[slot], r.eu.at[slot], r.ed.at[slot])
         return result.astype(bf16).astype(f32) * column
 
-    def arrive_piece(level, p):
-        @pl.when(level < z)
-        def _():
-            if p == 0:
-                gate_move(level, r.gate_up, below).wait_recv()
-            tok_move(level, p, r.tok_up, below).wait_recv()
-
-            @pl.when(not_last)
-            def _():
-                if p == 0:
-                    gate_move(level, r.gate_up, above).start()
-                tok_move(level, p, r.tok_up, above).start()
-
-        @pl.when(level > z)
-        def _():
-            if p == 0:
-                gate_move(level, r.gate_dn, above).wait_recv()
-            tok_move(level, p, r.tok_dn, above).wait_recv()
-
-            @pl.when(not_first)
-            def _():
-                if p == 0:
-                    gate_move(level, r.gate_dn, below).start()
-                tok_move(level, p, r.tok_dn, below).start()
-
-    def arrive(level):
-        for p in range(ROW_PIECES):
-            arrive_piece(level, p)
-
     def up_back(level, p):
         return remote(
             piece(r.ret_out.at[level], p), piece(r.up_in.at[level], p), r.ret_send.at[0], r.up_recv.at[level, p], above
@@ -475,31 +483,32 @@
             piece(r.ret_out.at[level], p), piece(r.dn_in.at[level], p), r.ret_send.at[0], r.dn_recv.at[level, p], below
         )
 
+    def give_piece(level, p):
+        span = pl.ds(p * part_rows, part_rows)
+
+        def send(back, came, chained):
+            @pl.when(chained)
+            def _():
+                back(level, p).wait_recv()
+                r.ret_out[level, span, :] = (r.own[level, span, :] + came[level, span, :].astype(f32)).astype(bf16)
+
+            @pl.when(jnp.logical_not(chained))
+            def _():
+                r.ret_out[level, span, :] = r.own[level, span, :].astype(bf16)
+
+            back(level, p).start()
+
+        @pl.when(level > z)
+        def _():
+            send(up_back, r.up_in, not_first)
+
+        @pl.when(level < z)
+        def _():
+            send(dn_back, r.dn_in, not_last)
+
     def give_back(level):
-        def send(back, came, chained):
-            for p in range(ROW_PIECES):
-                span = pl.ds(p * part_rows, part_rows)
-
-                @pl.when(chained)
-                def _():
-                    back(level, p).wait_recv()
-                    r.ret_out[level, span, :] = (
-                        r.own[level, span, :] + came[level, span, :].astype(f32)
-                    ).astype(bf16)
-
-                @pl.when(jnp.logical_not(chained))
-                def _():
-                    r.ret_out[level, span, :] = r.own[level, span, :].astype(bf16)
-
-                back(level, p).start()
-
-        @pl.when(level > z)
-        def _():
-            send(up_back, r.up_in, not_first)
-
-        @pl.when(level < z)
-        def _():
-            send(dn_back, r.dn_in, not_last)
+        for p in range(ROW_PIECES):
+            give_piece(level, p)
 
     def own_expert_on(level):
         r.own[level] = expert(level, 0, me)
@@ -508,34 +517,36 @@
         r.own[level] += expert(level, 1, mate_block)
 
     def first_turns(k, _):
-        level = jnp.where(k == 0, at_z(1, 0, 1, 2), jnp.where(k == 1, at_z(2, 2, 0, 1), z))
+        level = jnp.where(k == 0, at_z(1, 0, 0, 2), jnp.where(k == 1, at_z(2, 2, 1, 0), z))
 
         @pl.when(k < 2)
         def _():
             for p in range(ROW_PIECES):
-                arrive_piece(level, p)
+
+                @pl.when(jnp.logical_or(z != 1, k == 1))
+                def _():
+                    arrive_piece(level, p)
 
                 @pl.when(jnp.logical_and(z == last - 1, k == 1))
                 def _():
                     arrive_piece(last, p)
 
-            spread(jnp.where(k == 0, marks[3], marks[4]), jnp.where(k == 0, marks[4], PIECES))
+            spread(jnp.where(k == 0, marks[3], marks[4]), jnp.where(k == 0, marks[4], marks[5]))
 
         own_expert_on(level)
         return 0
 
     lax.fori_loop(0, 3, first_turns, 0)
     r.base[...] += gated(r.tok[z], r.sg, r.su, r.sd)
-
-    @pl.when(not_first)
-    def _():
-        level = at_z(0, 3, 3, 0)
-
-        @pl.when(z != last - 1)
-        def _():
-            arrive(level)
-
-        own_expert_on(level)
+    spread(marks[5], PIECES)
+
+    @pl.when(jnp.logical_and(not_first, not_last))
+    def _():
+        @pl.when(z == 1)
+        def _():
+            arrive(last)
+
+        own_expert_on(last)
 
     spread_x(x_mark, PIECES - EXTRA)
     for i in range(PIECES - EXTRA, PIECES):
@@ -544,50 +555,59 @@
     w_core_all().wait_recv()
 
     def second_turns(k, _):
-        level = jnp.where(k == line - 1, z, at_z(k + 1, pick(k, (3, 0, 2)), pick(k, (0, 3, 1)), k))
-
-        @pl.when(jnp.logical_and(z == 0, k == 2))
+        level = at_z(pick(k, (2, 1, 3)), pick(k, (2, 0, 3)), pick(k, (0, 1, 3)), k)
+
+        @pl.when(jnp.logical_or(jnp.logical_and(z == 0, k == 2), jnp.logical_and(z == last, k == 1)))
         def _():
             arrive(level)
             own_expert_on(level)
 
         mates_expert_on(level)
 
-        @pl.when(jnp.logical_or(jnp.logical_and(z == last, k < line - 1), jnp.logical_and(z == 0, k == 0)))
+        @pl.when(jnp.logical_or(z == last, jnp.logical_and(z == 0, k != 1)))
         def _():
             give_back(level)
 
-        @pl.when(jnp.logical_and(z == 0, k == 2))
-        def _():
-            give_back(last)
-            give_back(2)
-
         return 0
 
-    lax.fori_loop(0, line, second_turns, 0)
+    lax.fori_loop(0, line - 1, second_turns, 0)
+
+    give_back(at_z(1, 2, 0, z))
+    mates_expert_on(z)
     r.base[...] += r.own[z]
 
     @pl.when(jnp.logical_and(not_first, not_last))
     def _():
-        def middle(k, _):
-            give_back(at_z(0, pick(k, (3, 0, 2)), pick(k, (0, 3, 1)), 0))
-            return 0
-
-        lax.fori_loop(0, line - 1, middle, 0)
-
-    @pl.when(not_first)
-    def _():
-        for p in range(ROW_PIECES):
+        lag = 2
+        for step in range(ROW_PIECES + lag):
+
+            @pl.when(z == 1)
+            def _():
+                if step < ROW_PIECES:
+                    give_piece(0, step)
+                    give_piece(last, step)
+
+            @pl.when(z == last - 1)
+            def _():
+                if step < ROW_PIECES:
+                    give_piece(1, step)
+                if step >= lag:
+                    give_piece(last, step - lag)
+
+    for p in range(ROW_PIECES):
+        span = slice(p * part_rows, (p + 1) * part_rows)
+
+        @pl.when(not_first)
+        def _():
             up_back(z, p).wait_recv()
-        r.base[...] += r.up_in[z].astype(f32)
-
-    @pl.when(not_last)
-    def _():
-        for p in range(ROW_PIECES):
+            r.base[span, :] += r.up_in[z, span, :].astype(f32)
+
+        @pl.when(not_last)
+        def _():
             dn_back(z, p).wait_recv()
-        r.base[...] += r.dn_in[z].astype(f32)
-
-    r.out_ref[...] = r.base[...].astype(bf16)
+            r.base[span, :] += r.dn_in[z, span, :].astype(f32)
+
+        r.out_ref[span, :] = r.base[span, :].astype(bf16)
 
     for copy in side_moves(me, (r.fsend, r.ksend, r.vsend)) + [q_move(y), back_move(y, 0), back_move(y, 1)]:
         copy.wait_send()
@@ -649,7 +669,7 @@
     rows, width = residual.shape
     line = sp_count // 2
     bf16, f32 = jnp.bfloat16, jnp.float32
-    vmem, hbm = pl.BlockSpec(memory_space=pltpu.VMEM), pl.BlockSpec(memory_space=pl.ANY)
+    hbm = pl.BlockSpec(memory_space=pl.ANY)
     loaded = (
         out_weight,
         expert_gate[0],
@@ -741,9 +761,9 @@
     names = ins + ["out_ref"] + list(scratch)
     return pl.pallas_call(
         functools.partial(layer_kernel, names, sp_count, HEAD_DIM ** (-0.5)),
-        out_shape=jax.ShapeDtypeStruct(one, bf16),
+        out_shape=pltpu.VMEM(one, bf16),
         in_specs=[hbm] * 15,
-        out_specs=vmem,
+        out_specs=pl.BlockSpec(memory_space=pltpu.VMEM),
         scratch_shapes=list(scratch.values()),
         compiler_params=pltpu.CompilerParams(
             collective_id=0, has_side_effects=True, vmem_limit_bytes=60 * 2**20

time: 77.4 us -> 68.2 us (0.88)
  the two profiles are of different devices: /device:TPU:9 before, /device:TPU:24 now
where the time goes in v3:
time: 68.2 us; the launch traced here: 67.8 us
  Pallas kernels  67.1 us (98%)
  local copies, waits for them, and re-layouts  0.71 us (1%)
    pallas_call x1, Pallas kernels, layer_fused(): pl.pallas_call(functools.partial(layer_kernel, names, sp_count, HEAD_DIM...  67.1 us

profile of v3, /device:TPU:24, one launch (start us, length us, event | category | flops | bytes accessed | tf_op | source)
XLA Modules:
  0.0 67.8 jit_solution(1561610320605063382)
XLA Ops:
  0.0 67.1 %shard_map.145 = bf16[64,2048]{1,0:T(8,128)(2,1)S(1)} custom-call(bf16[256,512]{1,0:T(8,128)(2,1)} %refs_0_.1, f32[4,256]{1,0:T(4,128)} %bitcast.11, bf16[256,256]{1,0:T(8,128)(2,1)} %refs_2_.1, bf16[256,256]{1,0:T(8,128)(2,1)} %refs_3_.1, bf16[64,2048]{1,0:T(8,128)(2,1)} %refs_4_.1, f32[1,2048]{1,0:T(1,128)} %bitcast.10, s32[4,64]{1,0:T(4,128)} %bitcast.12, ...), custom_call_target="tpu_custom_call" | custom-call | tf_op jit(solution)/shard_map/pallas_call | solution.py:762
  67.1 0.7 %copy.17 = bf16[64,2048]{1,0:T(8,128)(2,1)} copy(bf16[64,2048]{1,0:T(8,128)(2,1)S(1)} %shard_map.145) | data formatting | bytes 524288

commit v4 on v3

--- a/solution.py
+++ b/solution.py
@@ -153,14 +153,15 @@
             for a, b in zip(parts(sources, quarter, i), parts(mates_expert, quarter, i))
         ]
 
-    piece_rows = 3 * (r.eg.shape[1] // 4 // PIECES)
-
-    def w_all(count, send, recv, target):
-        one = r.eg.at[1, 0 : count * piece_rows, :]
+    third = r.eg.shape[1] // 4 // PIECES
+    last_hop = PIECES - EXTRA - 1
+
+    def w_all(thirds, send, recv, target):
+        one = r.eg.at[1, 0 : thirds * third, :]
         return remote(one, one, send, recv, target)
 
     def w_core_all():
-        both = r.eg.at[:, 0 : PIECES * piece_rows, :]
+        both = r.eg.at[:, 0 : PIECES * 3 * third, :]
         return remote(both, both, r.wc_sem.at[0], r.wc_sem.at[1], core_mate)
 
     x_quarter = 2 * (1 - x) + c
@@ -174,9 +175,11 @@
         lax.fori_loop(start, stop, one, 0)
 
     def issue_extra():
+        by_y = w_moves(own_expert, x_quarter, last_hop, r.wy_send.at[0], r.wy_recv.at[PIECES], mate)[2:]
         for i in range(PIECES - EXTRA, PIECES):
-            for copy in w_moves(own_expert, x_quarter, i, r.wy_send.at[0], r.wy_recv.at[EXTRA + i], mate):
-                copy.start()
+            by_y += w_moves(own_expert, x_quarter, i, r.wy_send.at[0], r.wy_recv.at[EXTRA + i + 1], mate)
+        for copy in by_y:
+            copy.start()
 
     def to_core(i, quarter):
         for copy in w_moves(mates_expert, quarter, i, r.wc_sem.at[0], r.wc_sem.at[1], core_mate):
@@ -184,12 +187,18 @@
 
     def spread(start, stop):
         def one(i, _):
-            w_all(1, r.wy_send.at[0], r.wy_recv.at[i], mate).wait_recv()
-
-            @pl.when(i < PIECES - EXTRA)
+            w_all(3, r.wy_send.at[0], r.wy_recv.at[i], mate).wait_recv()
+
+            hops = w_moves(mates_expert, tp, i, r.wx_send.at[0], r.wx_recv.at[i], x_mate)
+
+            @pl.when(i <= last_hop)
             def _():
-                for copy in w_moves(mates_expert, tp, i, r.wx_send.at[0], r.wx_recv.at[i], x_mate):
+                for copy in hops[:2]:
                     copy.start()
+
+            @pl.when(i < last_hop)
+            def _():
+                hops[2].start()
 
             to_core(i, tp)
             return 0
@@ -198,7 +207,7 @@
 
     def spread_x(start, stop):
         def one(i, _):
-            w_all(1, r.wx_send.at[0], r.wx_recv.at[i], x_mate).wait_recv()
+            w_all(3, r.wx_send.at[0], r.wx_recv.at[i], x_mate).wait_recv()
             to_core(i, x_quarter)
             return 0
 
@@ -210,7 +219,7 @@
             out = jnp.where(z == level, values[level], out)
         return out
 
-    early = at_z(1, 2, 3, 5)
+    early = at_z(2, 2, 3, 5)
     for copy in side_moves(me, (r.fsend, r.ksend, r.vsend)):
         copy.start()
     pass_up(me)
@@ -343,7 +352,7 @@
         absorb(y, 1 - y, False)
 
     finish(y, r.att.at[y])
-    marks = [at_z(0, 1, 2, 3), at_z(1, 2, 3, 5), at_z(2, 3, 4, 6), at_z(6, 4, 6, 7), at_z(8, 6, 7, 8), at_z(8, 7, 8, 8)]
+    marks = [at_z(0, 1, 2, 3), at_z(2, 2, 3, 5), at_z(3, 3, 4, 6), at_z(6, 4, 6, 7), at_z(8, 6, 7, 8), at_z(8, 7, 8, 8)]
     x_mark = at_z(1, 2, 3, 4)
     spread(marks[0], marks[1])
 
@@ -440,10 +449,6 @@
         r.tok[z, span, :] = (wide * scale * r.gain_ref[...]).astype(bf16)
         r.base[span, :] = wide
 
-        @pl.when(z == 1)
-        def _():
-            arrive_piece(0, p)
-
         @pl.when(not_last)
         def _():
             tok_move(z, p, r.tok_up, above).start()
@@ -463,14 +468,15 @@
         hidden = (first / (1.0 + jnp.exp(-first)) * second).astype(bf16)
         return jnp.dot(hidden, down[...], preferred_element_type=f32)
 
-    def expert(level, slot, number):
+    def expert(level, slot, number, start, count):
         table = r.gbuf[level]
         at_expert = lax.broadcasted_iota(jnp.int32, table.shape, 0) == number
         row = jnp.sum(jnp.where(at_expert, table, 0.0), axis=0, keepdims=True)
-        shape = (rows, row.shape[1])
-        diagonal = lax.broadcasted_iota(jnp.int32, shape, 0) == lax.broadcasted_iota(jnp.int32, shape, 1)
+        shape = (count, row.shape[1])
+        diagonal = lax.broadcasted_iota(jnp.int32, shape, 0) + start == lax.broadcasted_iota(jnp.int32, shape, 1)
         column = jnp.sum(jnp.where(diagonal, row, 0.0), axis=1, keepdims=True)
-        result = gated(r.tok[level], r.eg.at[slot], r.eu.at[slot], r.ed.at[slot])
+        inputs = r.tok[level, pl.ds(start, count), :]
+        result = gated(inputs, r.eg.at[slot], r.eu.at[slot], r.ed.at[slot])
         return result.astype(bf16).astype(f32) * column
 
     def up_back(level, p):
@@ -511,68 +517,117 @@
             give_piece(level, p)
 
     def own_expert_on(level):
-        r.own[level] = expert(level, 0, me)
+        r.own[level] = expert(level, 0, me, 0, rows)
 
     def mates_expert_on(level):
-        r.own[level] += expert(level, 1, mate_block)
+        r.own[level] += expert(level, 1, mate_block, 0, rows)
 
     def first_turns(k, _):
-        level = jnp.where(k == 0, at_z(1, 0, 0, 2), jnp.where(k == 1, at_z(2, 2, 1, 0), z))
-
-        @pl.when(k < 2)
-        def _():
+        level = jnp.where(k == 0, at_z(1, 0, 0, 2), at_z(2, 2, 1, 0))
+
+        for p in range(ROW_PIECES):
+            arrive_piece(level, p)
+
+            @pl.when(jnp.logical_and(z == last - 1, k == 1))
+            def _():
+                arrive_piece(last, p)
+
+        spread(jnp.where(k == 0, marks[3], marks[4]), jnp.where(k == 0, marks[4], marks[5]))
+        own_expert_on(level)
+        return 0
+
+    at_end = jnp.logical_or(z == 0, z == last)
+
+    def self_turn():
+        own_expert_on(z)
+        r.base[...] += gated(r.tok[z], r.sg, r.su, r.sd)
+
+    @pl.when(at_end)
+    def _():
+        self_turn()
+
+    lax.fori_loop(0, 2, first_turns, 0)
+
+    @pl.when(jnp.logical_not(at_end))
+    def _():
+        self_turn()
+
+    spread(marks[5], PIECES)
+
+    @pl.when(jnp.logical_and(not_first, not_last))
+    def _():
+        @pl.when(z == 1)
+        def _():
+            arrive(last)
+
+        own_expert_on(last)
+
+    spread_x(x_mark, last_hop)
+    w_all(2, r.wx_send.at[0], r.wx_recv.at[last_hop], x_mate).wait_recv()
+    w_all(1, r.wy_send.at[0], r.wy_recv.at[PIECES], mate).wait_recv()
+    to_core(last_hop, x_quarter)
+    for i in range(PIECES - EXTRA, PIECES):
+        w_all(3, r.wy_send.at[0], r.wy_recv.at[EXTRA + i + 1], mate).wait_recv()
+        to_core(i, x_quarter)
+    w_core_all().wait_recv()
+
+    def second_turns(k, _):
+        level = at_z(pick(k, (2, 1, 3)), pick(k, (2, 0, 3)), pick(k, (0, 1, 3)), k)
+
+        @pl.when(jnp.logical_and(z == last, k == 1))
+        def _():
+            arrive(level)
+            own_expert_on(level)
+
+        mates_expert_on(level)
+
+        @pl.when(z == last)
+        def _():
+            give_back(level)
+
+        @pl.when(jnp.logical_and(z == 0, k == 0))
+        def _():
+            for p in range(ROW_PIECES // 2):
+                give_piece(level, p)
+
+        return 0
+
+    lax.fori_loop(0, jnp.where(z == 0, line - 2, line - 1), second_turns, 0)
+
+    @pl.when(z == 0)
+    def _():
+        def one_half(i, _):
+            start, count = i * (rows // 2), rows // 2
             for p in range(ROW_PIECES):
 
-                @pl.when(jnp.logical_or(z != 1, k == 1))
-                def _():
-                    arrive_piece(level, p)
-
-                @pl.when(jnp.logical_and(z == last - 1, k == 1))
+                @pl.when(p // (ROW_PIECES // 2) == i)
                 def _():
                     arrive_piece(last, p)
 
-            spread(jnp.where(k == 0, marks[3], marks[4]), jnp.where(k == 0, marks[4], marks[5]))
-
-        own_expert_on(level)
-        return 0
-
-    lax.fori_loop(0, 3, first_turns, 0)
-    r.base[...] += gated(r.tok[z], r.sg, r.su, r.sd)
-    spread(marks[5], PIECES)
-
-    @pl.when(jnp.logical_and(not_first, not_last))
-    def _():
-        @pl.when(z == 1)
-        def _():
-            arrive(last)
-
-        own_expert_on(last)
-
-    spread_x(x_mark, PIECES - EXTRA)
-    for i in range(PIECES - EXTRA, PIECES):
-        w_all(1, r.wy_send.at[0], r.wy_recv.at[EXTRA + i], mate).wait_recv()
-        to_core(i, x_quarter)
-    w_core_all().wait_recv()
-
-    def second_turns(k, _):
-        level = at_z(pick(k, (2, 1, 3)), pick(k, (2, 0, 3)), pick(k, (0, 1, 3)), k)
-
-        @pl.when(jnp.logical_or(jnp.logical_and(z == 0, k == 2), jnp.logical_and(z == last, k == 1)))
-        def _():
-            arrive(level)
-            own_expert_on(level)
-
-        mates_expert_on(level)
-
-        @pl.when(jnp.logical_or(z == last, jnp.logical_and(z == 0, k != 1)))
-        def _():
-            give_back(level)
-
-        return 0
-
-    lax.fori_loop(0, line - 1, second_turns, 0)
-
-    give_back(at_z(1, 2, 0, z))
+            both = expert(last, 0, me, start, count) + expert(last, 1, mate_block, start, count)
+            r.own[last, pl.ds(start, count), :] = both
+            for p in range(ROW_PIECES):
+
+                @pl.when(p // (ROW_PIECES // 2) == i)
+                def _():
+                    give_piece(last, p)
+
+            return 0
+
+        lax.fori_loop(0, 2, one_half, 0)
+        for p in range(ROW_PIECES // 2, ROW_PIECES):
+            give_piece(last - 1, p)
+
+
+    @pl.when(z != 1)
+    def _():
+        give_back(at_z(1, 1, 0, z))
+
+    @pl.when(z == 1)
+    def _():
+        for p in range(ROW_PIECES // 2):
+            give_piece(2, p)
+
     mates_expert_on(z)
     r.base[...] += r.own[z]
 
@@ -586,6 +641,8 @@
                 if step < ROW_PIECES:
                     give_piece(0, step)
                     give_piece(last, step)
+                else:
+                    give_piece(2, step - ROW_PIECES // 2)
 
             @pl.when(z == last - 1)
             def _():
@@ -617,8 +674,8 @@
         remote(whole, whole, send, recv, target).wait_send()
 
     sent(r.x_out, r.hop_send.at[0], r.hop_recv.at[0], x_mate)
-    w_all(PIECES + EXTRA, r.wy_send.at[0], r.wy_recv.at[0], mate).wait_send()
-    w_all(PIECES - EXTRA, r.wx_send.at[0], r.wx_recv.at[0], x_mate).wait_send()
+    w_all(3 * (PIECES + EXTRA) + 1, r.wy_send.at[0], r.wy_recv.at[0], mate).wait_send()
+    w_all(3 * (PIECES - EXTRA) - 1, r.wx_send.at[0], r.wx_recv.at[0], x_mate).wait_send()
     w_core_all().wait_send()
     done = pl.ds(0, line - 1)
 
@@ -741,7 +798,7 @@
         "back_send": dma(2),
         "back_recv": dma(2),
         "wy_send": dma(1),
-        "wy_recv": dma(PIECES + EXTRA),
+        "wy_recv": dma(PIECES + EXTRA + 1),
         "wx_send": dma(1),
         "wx_recv": dma(PIECES),
         "wc_sem": dma(2),

time: 68.2 us -> 66.9 us (0.981)
  Pallas kernels: 67.1 us -> 65.3 us
    pallas_call x1, Pallas kernels: 67.1 us -> 65.3 us  [layer_fused(): pl.pallas_call(functools.partial(layer_kernel, names, sp_count, HEAD_DIM...]
where the time goes in v4:
time: 66.9 us; the launch traced here: 66 us
  Pallas kernels  65.3 us (98%)
  local copies, waits for them, and re-layouts  0.71 us (1%)
    pallas_call x1, Pallas kernels, layer_fused(): pl.pallas_call(functools.partial(layer_kernel, names, sp_count, HEAD_DIM...  65.3 us

profile of v4, /device:TPU:24, one launch (start us, length us, event | category | flops | bytes accessed | tf_op | source)
XLA Modules:
  0.0 66.0 jit_solution(13982168755777225218)
XLA Ops:
  0.0 65.3 %shard_map.145 = bf16[64,2048]{1,0:T(8,128)(2,1)S(1)} custom-call(bf16[256,512]{1,0:T(8,128)(2,1)} %refs_0_.1, f32[4,256]{1,0:T(4,128)} %bitcast.11, bf16[256,256]{1,0:T(8,128)(2,1)} %refs_2_.1, bf16[256,256]{1,0:T(8,128)(2,1)} %refs_3_.1, bf16[64,2048]{1,0:T(8,128)(2,1)} %refs_4_.1, f32[1,2048]{1,0:T(1,128)} %bitcast.10, s32[4,64]{1,0:T(4,128)} %bitcast.12, ...), custom_call_target="tpu_custom_call" | custom-call | tf_op jit(solution)/shard_map/pallas_call | solution.py:819
  65.3 0.7 %copy.17 = bf16[64,2048]{1,0:T(8,128)(2,1)} copy(bf16[64,2048]{1,0:T(8,128)(2,1)S(1)} %shard_map.145) | data formatting | bytes 524288
